TPU v7x, 256 devices: a whole 4x4x8 slice. The times are simulated.
256 devices in a mesh: rep: 2 (over z_hi), fs: 16 (over z_lo, x), tp: 8 (over y, core).
Axes of the slice: x: 4, y: 4, z: 8 (z_hi: 2, z_lo: 4; z = z_hi * 4 + z_lo), core: 2. Of those that a mesh axis runs over, the one named last changes fastest.
Arguments:
- stream: bfloat16 [32768, 2048], P(('rep', 'fs', 'tp')), may hold values from -6 to 6
- gate_weight: bfloat16 [2048, 2816], P('fs', 'tp'), may hold values from -0.125 to 0.125
- up_weight: bfloat16 [2048, 2816], P('fs', 'tp'), may hold values from -0.125 to 0.125
- down_weight: bfloat16 [2816, 2048], P('tp', 'fs'), may hold values from -0.21875 to 0.21875
- query_weight: bfloat16 [2048, 512], P('fs', 'tp'), may hold values from -0.125 to 0.125
- key_weight: bfloat16 [2048, 512], P('fs', 'tp'), may hold values from -0.125 to 0.125
- value_weight: bfloat16 [2048, 1024], P('fs', 'tp'), may hold values from -0.125 to 0.125
- outgate_weight: bfloat16 [2048, 1024], P('fs', 'tp'), may hold values from -0.125 to 0.125
- decay_down: bfloat16 [2048, 32], replicated, may hold values from -0.125 to 0.125
- decay_up: bfloat16 [32, 512], P(None, 'tp'), may hold values from -2 to 2
- decay_bias: float32 [512], P('tp'), may hold values from -0.5 to 7
- head_gain: float32 [128], replicated, may hold values from 0.1 to 1.9
- out_weight: bfloat16 [1024, 2048], P('tp', 'fs'), may hold values from -0.375 to 0.375
- norm_gain: float32 [3, 2048], replicated, may hold values from 0.1 to 1.9
Outputs:
- layer_out: bfloat16 [32768, 2048], P(('rep', 'fs', 'tp'))
All inputs are finite; a program needn't handle non-finite values.
Results may differ from a plain program's by a relative error of at most 0.015.
Values may be sent and summed in bfloat16 or wider, within the bound.
No kernel may reach another device: no remote copies, remote signals or barrier semaphores. Data moves between devices by JAX's collectives and lax.ppermute only.
A program may use at most 128 MiB of HBM per device.

v0:
```python
import jax
import jax.numpy as jnp
import numpy as np
from jax import lax
from jax.experimental import pallas as pl
from jax.experimental.pallas import tpu as pltpu
from jax.sharding import Mesh, PartitionSpec as P


DK = 64
DV = 128
ROWS = 256
D = 2048
HID = 352
LANE = 128
HEADS = 4
MIX = 352
TAIL = 32
LEVELS = 8

RESIDUAL_SCALE = 2.0**0.5
BRANCH_SCALE = 0.5
NORM_EPS = 1e-05
HEAD_EPS = 0.01
GATE_DIVISOR = 16.0

F32 = jnp.float32
BF16 = jnp.bfloat16
LARGE = ("zxy", "yzx")
SMALL = ("xyz", "xyz")
AXES = {"r": 2, "z": 4, "x": 4, "y": 4, "c": 2}
VMEM_LIMIT = 20 * 1024 * 1024


def shifted(value, axes, step):
    pairs = []
    for n in range(256):
        r, z, x, y, c = (int(i) for i in np.unravel_index(n, tuple(AXES.values())))
        axis = axes[c]
        if axis == "z":
            ring = 4 * r + z
            go = -step if step == 2 and ring % 2 else step
            r, z = divmod((ring - go) % 8, 4)
        elif axis == "x":
            x = (x - step) % 4
        else:
            y = (y - step) % 4
        pairs.append((n, int(np.ravel_multi_index((r, z, x, y, c), tuple(AXES.values())))))
    return lax.ppermute(value, tuple(AXES), pairs)


def gathered_direct(value, axis):
    ahead, behind = shifted(value, axis, 1), shifted(value, axis, -1)
    return [value, ahead, shifted(value, axis, 2), behind]


def gathered_ring(low, high, axis):
    ahead_low, behind_low = shifted(low, axis, 1), shifted(low, axis, -1)
    behind_high, ahead_high = shifted(high, axis, -1), shifted(high, axis, 1)
    far_low = shifted(ahead_low, axis, 1)
    far_high = shifted(behind_high, axis, -1)
    return [low, high, ahead_low, ahead_high, far_low, far_high, behind_low, behind_high]


def gathered_planes(value, orders):
    first, second, _ = zip(*orders)
    line = gathered_direct(value, first)
    line = call(stack_kernel, [((4, *value.shape), BF16)], [], line)[0]
    return gathered_direct(line, second)


def last_of(orders):
    return tuple(order[2] for order in orders)


def fs_block(place_ref, dz, dx):
    return ((place_ref[0] + dz) % 4) * 4 + (place_ref[1] + dx) % 4


def normed(values, gain):
    average = jnp.mean(values, -1, keepdims=True)
    centred = values - average
    spread = jnp.mean(centred * centred, -1, keepdims=True)
    return (centred * lax.rsqrt(spread + NORM_EPS) * gain).astype(BF16)


def after_branch(out_ref, base_ref, mine_ref, other_ref, gain_ref, scale):
    @pl.loop(0, out_ref.shape[0] // 64)
    def _(n):
        rows = pl.ds(pl.multiple_of(n * 64, 64), 64)
        branch = mine_ref[rows, :].astype(F32) + other_ref[rows, :].astype(F32)
        out_ref[rows, :] = normed(RESIDUAL_SCALE * base_ref[rows, :].astype(F32) + scale * branch, gain_ref[...])


def dot_t(a, b):
    return lax.dot_general(a, b, (((1,), (1,)), ((), ())), preferred_element_type=F32)


def ordered_columns(place_ref, ref):
    blocks = []
    for dx in range(4):
        for dz in range(4):
            blocks.append(ref[:, pl.ds(pl.multiple_of(fs_block(place_ref, dz, dx) * LANE, LANE), LANE)])
    return jnp.concatenate(blocks, axis=1)


def joined_features(block):
    return jnp.concatenate([block(dx, dz) for dx in range(4) for dz in range(4)], axis=1)


def prepare_kernel(gate_ref, up_ref, query_ref, key_ref, value_ref, outgate_ref, down_ref, out_ref, *refs):
    large, small, value, outgate, sem = refs
    row, copies = 0, []
    for ref in (gate_ref, up_ref, query_ref, key_ref):
        copies.append((ref, large.at[pl.ds(row, ref.shape[0])]))
        row += ref.shape[0]
    copies += [(down_ref, small.at[pl.ds(0, HID)]), (out_ref, small.at[pl.ds(HID + TAIL, DV)])]
    copies += [(value_ref, value), (outgate_ref, outgate)]
    copies = [pltpu.make_async_copy(*pair, sem.at[n]) for n, pair in enumerate(copies)]
    for copy in copies:
        copy.start()
    for copy in copies:
        copy.wait()
    large[row : row + DV, :] = value[...].astype(F32).T.astype(BF16)
    turned = outgate[...].astype(F32).T.astype(BF16)
    large[row + DV :, :] = turned[: DV - TAIL]
    small[HID : HID + TAIL, :] = turned[DV - TAIL :]


def stack_kernel(*refs):
    for n in range(4):
        refs[4][n] = refs[n][...]


def divide_low_kernel(plane, ahead, low):
    units = low.shape[2]
    low[0] = plane[:, :units]
    low[1] = ahead[:, :units]


def divide_high_kernel(*refs):
    planes, (high, mix) = refs[:4], refs[4:]
    units = high.shape[2]
    for n, plane in enumerate(planes):
        if n > 1:
            high[n - 2] = plane[:, :units]
        mix[n] = plane[:, units:]


def arranged(place_ref, pieces, halves, y, dst):
    inner = 4 // halves
    for k in range(4):

        @pl.when((place_ref[2] == 0) & (y == k))
        def _():
            for half in range(halves):

                @pl.loop(0, inner)
                def _(n):
                    for dz in range(4):
                        dst[half * inner + n, dz] = pieces[halves * k + half][n, dz]

    @pl.when(place_ref[2] == 1)
    def _():
        for dx in range(4):
            for half in range(halves):

                @pl.loop(0, inner)
                def _(n):
                    dst[dx, half * inner + n] = pieces[halves * dx + half][n, y]


def hidden_units(x, large, y, hidden):
    both = dot_t(x, joined_features(lambda dx, dz: large[y, dx, dz]))
    gate, upward = both[:, :HID], both[:, HID:]
    hidden[y] = (gate / (1.0 + jnp.exp(-gate)) * upward).astype(BF16)


def projected(place_ref, units, block, store):
    @pl.loop(0, 4)
    def _(dx):
        columns = [jnp.concatenate([block(dz, y, dx) for y in range(4)], axis=0) for dz in range(4)]
        part = jnp.dot(units(), jnp.concatenate(columns, axis=1), preferred_element_type=F32).astype(BF16)
        for dz in range(4):
            column = pl.multiple_of(fs_block(place_ref, dz, dx) * LANE, LANE)
            store(pl.ds(column, LANE), part[:, dz * LANE : (dz + 1) * LANE])


def ffn_first_kernel(place_ref, x_ref, *refs):
    large_p, small_p = refs[:8], refs[8:16]
    out_ref, large_ref, hidden = refs[16:]
    x = ordered_columns(place_ref, x_ref)

    @pl.loop(0, 4)
    def _(y):
        arranged(place_ref, large_p, 2, y, large_ref.at[y])
        hidden_units(x, large_ref, y, hidden)

    def store(columns, value):
        out_ref[:, columns] = value

    projected(
        place_ref,
        lambda: jnp.concatenate([hidden[y] for y in range(4)], axis=1),
        lambda dz, y, dx: small_p[2 * dz + y // 2][y % 2, dx],
        store,
    )


def ffn_second_kernel(place_ref, base_ref, mine_ref, other_ref, gain_ref, large_ref, *refs):
    small_p = refs[:8]
    own_ref, keep_ref, give_ref, hidden, second = refs[8:]
    core = place_ref[2]
    after_branch(second, base_ref, mine_ref, other_ref, gain_ref, 1.0)
    own_ref[...] = second[pl.ds(pl.multiple_of(core * 128, 128), 128), :]
    x = ordered_columns(place_ref, second)

    @pl.loop(0, 4)
    def _(y):
        hidden_units(x, large_ref, y, hidden)

    def store(columns, value):
        keep_ref[:, columns] = jnp.where(core == 0, value[:128], value[128:])
        give_ref[:, columns] = jnp.where(core == 0, value[128:], value[:128])

    projected(
        place_ref,
        lambda: jnp.concatenate([hidden[y] for y in range(4)], axis=1),
        lambda dz, y, dx: small_p[2 * dz + y // 2][y % 2, dx],
        store,
    )


def last_norm_kernel(base_ref, mine_ref, other_ref, gain_ref, out_ref):
    after_branch(out_ref, base_ref, mine_ref, other_ref, gain_ref, BRANCH_SCALE)


FFN_SCRATCH = (pltpu.VMEM((4, ROWS, HID), BF16),)


def position_masks():
    t = lax.broadcasted_iota(jnp.int32, (ROWS, ROWS), 0)
    s = lax.broadcasted_iota(jnp.int32, (ROWS, ROWS), 1)
    return t, s


def summed(mask, high, low):
    ones = jnp.where(mask, 1.0, 0.0).astype(BF16)
    return jnp.dot(ones, high, preferred_element_type=F32) + jnp.dot(ones, low, preferred_element_type=F32)


def project_kernel(place_ref, base_ref, mine_ref, other_ref, gain_ref, down_ref, up_ref, bias_ref, *refs):
    first_ref, q_ref, k_ref, v_ref, outgate_ref, ghi_ref, glo_ref, state_ref, parts, large = refs[8:]
    large_p, small_p = refs[:4], refs[4:8]
    after_branch(first_ref, base_ref, mine_ref, other_ref, gain_ref, BRANCH_SCALE)
    first = first_ref[...]
    low = dot_t(first, down_ref[...]).astype(BF16)
    pre = jnp.dot(low, up_ref[...], preferred_element_type=F32) + bias_ref[...]
    log_gate = (jnp.minimum(pre, 0.0) - jnp.log1p(jnp.exp(-jnp.abs(pre)))) / GATE_DIVISOR
    ghi = log_gate.astype(BF16)
    glo = (log_gate - ghi.astype(F32)).astype(BF16)
    ghi_ref[...] = ghi
    glo_ref[...] = glo
    x = ordered_columns(place_ref, first_ref)

    @pl.loop(0, 4)
    def _(y):
        arranged(place_ref, large_p, 1, y, large)
        rows = [
            joined_features(lambda dx, dz: large[dx, dz]),
            joined_features(lambda dx, dz: small_p[dz][y, dx, :TAIL]),
        ]
        parts[y] = dot_t(x, jnp.concatenate(rows, axis=0)).astype(BF16)

    queries, keys = [], []
    for y in range(4):
        queries.append(parts[y, :, :DK])
        keys.append(parts[y, :, DK : 2 * DK])
        v_ref[:, pl.ds(y * DV, DV)] = parts[y, :, 2 * DK : 2 * DK + DV]
        outgate_ref[:, pl.ds(y * DV, DV)] = parts[y, :, 2 * DK + DV :]
    q_ref[...] = jnp.concatenate(queries, axis=1)
    k_ref[...] = jnp.concatenate(keys, axis=1)
    k32 = k_ref[...].astype(F32)
    t, s = position_masks()
    since = summed(s <= t, ghi, glo)
    until = summed(s > t, ghi, glo)
    kept = k32 * jnp.exp(until)
    q_ref[...] = q_ref[...] * jnp.asarray(DK**-0.5, BF16)
    head = lax.broadcasted_iota(jnp.int32, (ROWS, HEADS * DK), 1) // DK
    state = jnp.zeros((DV, HEADS * DK), F32)
    for h in range(HEADS):
        state += lax.dot_general(
            v_ref[:, h * DV : (h + 1) * DV],
            jnp.where(head == h, kept, 0.0).astype(BF16),
            (((0,), (0,)), ((), ())),
            preferred_element_type=F32,
        )
    state_ref[:DV, :] = state
    state_ref[DV:, :] = jnp.broadcast_to(since[ROWS - 1 :, :], (8, HEADS * DK))


def inside_kernel(q_ref, k_ref, v_ref, ghi_ref, glo_ref, mixed_ref, scores):
    q32 = q_ref[...].astype(F32)
    k32 = k_ref[...].astype(F32)
    head = lax.broadcasted_iota(jnp.int32, (ROWS, HEADS * DK), 1) // DK
    t, s = position_masks()

    def products(qs, ks):
        stacked = jnp.concatenate([jnp.where(head == h, qs, 0.0).astype(BF16) for h in range(HEADS)], axis=0)
        return dot_t(stacked, ks.astype(BF16))

    same = products(q32, k32)
    for h in range(HEADS):
        rows = pl.ds(h * ROWS, ROWS)
        scores[rows, :] = jnp.where(t == s, same[h * ROWS : (h + 1) * ROWS], 0.0)

    @pl.loop(0, LEVELS)
    def _(n):
        tn, sn = t >> n, s >> n
        upper = (tn & 1) == 1
        gap = summed((tn == sn) & ((upper & (s <= t)) | (~upper & (s > t))), ghi_ref[...], glo_ref[...])
        scale = jnp.exp(gap)
        part = products(q32 * scale, k32 * scale)
        chosen = upper & (tn == sn + 1)
        for h in range(HEADS):
            rows = pl.ds(h * ROWS, ROWS)
            scores[rows, :] = jnp.where(chosen, part[h * ROWS : (h + 1) * ROWS], scores[rows, :])

    for h in range(HEADS):
        columns = pl.ds(h * DV, DV)
        mixed_ref[:, columns] = jnp.dot(
            scores[pl.ds(h * ROWS, ROWS), :].astype(BF16), v_ref[:, columns], preferred_element_type=F32
        )


def output_kernel(
    place_ref, mixed_ref, q_ref, ghi_ref, glo_ref, outgate_ref, gain_ref, s1_ref, s2_ref, s3_ref, *refs
):
    (out_ref,) = refs[4:]
    states = [
        pltpu.roll(ref[...], (HEADS - back) * DK, axis=1) for back, ref in ((1, s1_ref), (2, s2_ref), (3, s3_ref))
    ]
    decay = [s[DV : DV + 1, :] for s in states]
    entering = (
        states[0][:DV]
        + jnp.exp(decay[0]) * states[1][:DV]
        + jnp.exp(decay[0] + decay[1]) * states[2][:DV]
    ).astype(BF16)
    t, s = position_masks()
    since = summed(s <= t, ghi_ref[...], glo_ref[...])
    scaled = q_ref[...].astype(F32) * jnp.exp(since)
    head = lax.broadcasted_iota(jnp.int32, (ROWS, HEADS * DK), 1) // DK
    gated = []
    for h in range(HEADS):
        columns = pl.ds(h * DV, DV)
        mixed = mixed_ref[:, columns] + dot_t(jnp.where(head == h, scaled, 0.0).astype(BF16), entering)
        size = jnp.mean(mixed * mixed, -1, keepdims=True)
        opened = outgate_ref[:, columns].astype(F32)
        opened = opened / (1.0 + jnp.exp(-opened))
        gated.append((mixed * lax.rsqrt(size + HEAD_EPS) * gain_ref[...] * opened).astype(BF16))
    channels = jnp.concatenate(gated, axis=1)

    def store(columns, value):
        out_ref[:, columns] = value

    projected(place_ref, lambda: channels, lambda dz, y, dx: refs[dz][y, dx, TAIL:], store)


def call(kernel, outs, scalars, arrays, scratch=(), flops=1_000_000, space=pltpu.VMEM):
    if space != pltpu.VMEM:
        arrays = [pltpu.with_memory_space_constraint(array, space) for array in arrays]
    in_specs = [pl.BlockSpec(memory_space=pltpu.SMEM)] * len(scalars) + [
        pl.BlockSpec(memory_space=space)
    ] * len(arrays)
    return pl.pallas_call(
        kernel,
        out_shape=[jax.ShapeDtypeStruct(*out) for out in outs],
        in_specs=in_specs,
        out_specs=[pl.BlockSpec(memory_space=pltpu.VMEM)] * len(outs),
        scratch_shapes=scratch,
        compiler_params=pltpu.CompilerParams(vmem_limit_bytes=VMEM_LIMIT),
        cost_estimate=pl.CostEstimate(flops=flops, bytes_accessed=1_000_000, transcendentals=0),
    )(*scalars, *arrays)


def on_device(
    stream,
    gate_weight,
    up_weight,
    down_weight,
    query_weight,
    key_weight,
    value_weight,
    outgate_weight,
    decay_down,
    decay_up,
    decay_bias,
    head_gain,
    out_weight,
    norm_gain,
):
    core = lax.axis_index("c")
    place = jnp.stack([lax.axis_index("z"), lax.axis_index("x"), core]).astype(jnp.int32)

    def swapped(value):
        return lax.ppermute(value, "c", [(0, 1), (1, 0)])

    other = swapped(stream)
    rows = jnp.where(core == 0, jnp.concatenate([stream, other]), jnp.concatenate([other, stream]))

    large, small = call(
        prepare_kernel,
        [((2 * HID + MIX, LANE), BF16), ((HID + TAIL + DV, LANE), BF16)],
        [],
        [
            gate_weight.T,
            up_weight.T,
            query_weight.T,
            key_weight.T,
            value_weight,
            outgate_weight,
            down_weight,
            out_weight,
        ],
        [pltpu.VMEM((LANE, DV), BF16), pltpu.VMEM((LANE, DV), BF16), pltpu.SemaphoreType.DMA((8,))],
        space=pltpu.HBM,
    )
    flat_ffn, flat_mix = [], []
    for shard, orders, units in ((small, SMALL, HID), (large, LARGE, 2 * HID)):
        planes = gathered_planes(shard, orders)
        rest = shard.shape[0] - units
        half = ((2, 4, units, LANE), BF16)
        (low,) = call(divide_low_kernel, [half], [], planes[:2])
        high, mix = call(divide_high_kernel, [half, ((4, 4, rest, LANE), BF16)], [], planes)
        flat_ffn = gathered_ring(low, high, last_of(orders)) + flat_ffn
        flat_mix = gathered_direct(mix, last_of(orders)) + flat_mix
    decay = jnp.concatenate(
        [decay_up.astype(F32), decay_bias[None, :], jnp.zeros((7, DK), F32)], axis=0
    )
    shifts = [shifted(decay, "yy", k) for k in (1, 2, 3)]
    decay = jnp.concatenate([decay, *shifts], axis=1)

    rows, decay_rows, decay_bias_row = lax.optimization_barrier((rows, decay[:32].astype(BF16), decay[32:33]))
    part, large = call(
        ffn_first_kernel,
        [((ROWS, D), BF16), ((4, 4, 4, 2 * HID, LANE), BF16)],
        [place],
        [rows, *flat_ffn],
        FFN_SCRATCH,
        4_400_000_000,
    )
    wide = ((ROWS, HEADS * DK), BF16)
    broad = ((ROWS, HEADS * DV), BF16)
    first, query, keys, values, outgate, ghi, glo, state = call(
        project_kernel,
        [((ROWS, D), BF16), wide, wide, broad, broad, wide, wide, ((DV + 8, HEADS * DK), F32)],
        [place],
        [
            rows,
            part,
            swapped(part),
            norm_gain[0:1],
            decay_down.T,
            decay_rows,
            decay_bias_row,
            *flat_mix,
        ],
        [pltpu.VMEM((4, ROWS, MIX + TAIL), BF16), pltpu.VMEM((4, 4, MIX, LANE), BF16)],
        2_000_000_000,
    )
    earlier = [
        lax.ppermute(state, "y", [(i, i + back) for i in range(4 - back)]) for back in (1, 2, 3)
    ]
    (mixed,) = call(
        inside_kernel,
        [((ROWS, HEADS * DV), F32)],
        [],
        [query, keys, values, ghi, glo],
        [pltpu.VMEM((HEADS * ROWS, ROWS), F32)],
        4_000_000_000,
    )
    (part,) = call(
        output_kernel,
        [((ROWS, D), BF16)],
        [place],
        [mixed, query, ghi, glo, outgate, head_gain[None, :], *earlier, *flat_mix[4:]],
        (),
        1_000_000_000,
    )
    own, keep, give = call(
        ffn_second_kernel,
        [((128, D), BF16)] * 3,
        [place],
        [first, part, swapped(part), norm_gain[1:2], large, *flat_ffn[8:]],
        [*FFN_SCRATCH, pltpu.VMEM((ROWS, D), BF16)],
        4_400_000_000,
    )
    (out,) = call(last_norm_kernel, [((128, D), BF16)], [], [own, keep, swapped(give), norm_gain[2:3]])
    return out


def solution(mesh):
    fine = Mesh(mesh.devices.reshape(2, 4, 4, 4, 2), ("r", "z", "x", "y", "c"))
    fs, tp = ("z", "x"), ("y", "c")
    in_specs = (
        P(("r", *fs, *tp), None),
        P(fs, tp),
        P(fs, tp),
        P(tp, fs),
        P(fs, tp),
        P(fs, tp),
        P(fs, tp),
        P(fs, tp),
        P(),
        P(None, tp),
        P(tp),
        P(),
        P(tp, fs),
        P(),
    )
    return jax.shard_map(on_device, mesh=fine, in_specs=in_specs, out_specs=P(("r", *fs, *tp), None), check_vma=False)
```

profile of v0, /device:TPU:1, one launch (start us, length us, event | category | flops | bytes accessed | tf_op | source)
XLA Modules:
  0.0 233.7 jit_solution(904213021315502688)
XLA Ops:
  0.0 1.2 shard_map.136
  1.2 3.6 %collective-permute-start.4 = (bf16[1056,128]{1,0:T(8,128)(2,1)S(1)}, bf16[1056,128]{1,0:T(8,128)(2,1)S(1)}, u32[]{:S(2)}, u32[]{:S(2)}) collective-permute-start(bf16[1056,128]{1,0:T(8,128)(2,1)S(1)} %get-tuple-element.28.refs_0_), channel_id=1, source_target_pairs={{0,224},{1,7},{2,226},{3,1},{4,228},{5,3},{6,230},{7,5},{8,232},{9... | collective-permute-start | bytes 811016 | tf_op jit(solution)/shard_map/ppermute | solution.py:49
  5.9 2.5 %collective-permute-start.16 = (bf16[512,128]{1,0:T(8,128)(2,1)S(1)}, bf16[512,128]{1,0:T(8,128)(2,1)S(1)}, u32[]{:S(2)}, u32[]{:S(2)}) collective-permute-start(bf16[512,128]{1,0:T(8,128)(2,1)S(1)} %get-tuple-element.30.refs_0_), channel_id=1, source_target_pairs={{0,24},{1,25},{2,26},{3,27},{4,28},{5,29},{6,30},{7,31},{8,0},{9,1... | collective-permute-start | bytes 393224 | tf_op jit(solution)/shard_map/ppermute | solution.py:49
  8.9 2.3 collective-permute-done.4.refs_1_
  11.1 1.2 collective-permute-start.18
  12.3 2.5 %collective-permute-done.6.refs_3_ = bf16[1056,128]{1,0:T(8,128)(2,1)S(1)} collective-permute-done((bf16[1056,128]{1,0:T(8,128)(2,1)S(1)}, bf16[1056,128]{1,0:T(8,128)(2,1)S(1)}, u32[]{:S(2)}, u32[]{:S(2)}) %collective-permute-start.6) | collective-permute-done | bytes 270368 | tf_op jit(solution)/shard_map/ppermute | solution.py:49
  14.9 5.4 %collective-permute-start.7 = (bf16[4,1056,128]{2,1,0:T(8,128)(2,1)S(1)}, bf16[4,1056,128]{2,1,0:T(8,128)(2,1)S(1)}, u32[]{:S(2)}, u32[]{:S(2)}) collective-permute-start(bf16[4,1056,128]{2,1,0:T(8,128)(2,1)S(1)} %shard_map.137.plane.refs_0_), channel_id=1, source_target_pairs={{0,24},{1,225},{2,26},{3,227},{4,28},{5,229},{6,30},{7,231},{8,0},... | collective-permute-start | bytes 3244040 | tf_op jit(solution)/shard_map/ppermute | solution.py:49
  20.3 1.5 collective-permute-start.8
  21.8 1.0 collective-permute-start.19
  22.8 12.0 %collective-permute-done.19.ahead.refs_1_ = bf16[4,512,128]{2,1,0:T(8,128)(2,1)S(1)} collective-permute-done((bf16[4,512,128]{2,1,0:T(8,128)(2,1)S(1)}, bf16[4,512,128]{2,1,0:T(8,128)(2,1)S(1)}, u32[]{:S(2)}, u32[]{:S(2)}) %collective-permute-start.19) | collective-permute-done | bytes 524320 | tf_op jit(solution)/shard_map/ppermute | solution.py:49
  35.1 12.1 %collective-permute-done.21.refs_3_ = bf16[4,512,128]{2,1,0:T(8,128)(2,1)S(1)} collective-permute-done((bf16[4,512,128]{2,1,0:T(8,128)(2,1)S(1)}, bf16[4,512,128]{2,1,0:T(8,128)(2,1)S(1)}, u32[]{:S(2)}, u32[]{:S(2)}) %collective-permute-start.21) | collective-permute-done | bytes 524320 | tf_op jit(solution)/shard_map/ppermute | solution.py:49
  47.3 3.2 %collective-permute-start.25 = (bf16[2,4,352,128]{3,2,1,0:T(8,128)(2,1)S(1)}, bf16[2,4,352,128]{3,2,1,0:T(8,128)(2,1)S(1)}, u32[]{:S(2)}, u32[]{:S(2)}) collective-permute-start(bf16[2,4,352,128]{3,2,1,0:T(8,128)(2,1)S(1)} %get-tuple-element.31.refs_9_.refs_1_), channel_id=1, source_target_pairs={{0,32},{1,33},{2,34},{3,35},{4,36},{5,37},{6,38},{7,39},{8,40},{9,... | collective-permute-start | bytes 2162696 | tf_op jit(solution)/shard_map/ppermute | solution.py:49
  50.6 1.3 shard_map.139
  51.9 0.9 collective-permute-start.13
  53.0 4.5 %collective-permute-start.10 = (bf16[2,4,704,128]{3,2,1,0:T(8,128)(2,1)S(1)}, bf16[2,4,704,128]{3,2,1,0:T(8,128)(2,1)}, u32[]{:S(2)}, u32[]{:S(2)}) collective-permute-start(bf16[2,4,704,128]{3,2,1,0:T(8,128)(2,1)S(1)} %shard_map.138.refs_0_), channel_id=1, source_target_pairs={{0,6},{1,25},{2,0},{3,27},{4,2},{5,29},{6,4},{7,31},{8,14},{9,1},{... | collective-permute-start | bytes 4325384 | tf_op jit(solution)/shard_map/ppermute | solution.py:49
  58.2 3.2 %collective-permute-done.1 = f32[40,64]{1,0:T(8,128)S(1)} collective-permute-done((f32[40,64]{1,0:T(8,128)S(1)}, f32[40,64]{1,0:T(8,128)S(1)}, u32[]{:S(2)}, u32[]{:S(2)}) %collective-permute-start.1) | collective-permute-done | bytes 10272 | tf_op jit(solution)/shard_map/ppermute | solution.py:49
  61.5 4.4 %collective-permute-done.2 = f32[40,64]{1,0:T(8,128)S(1)} collective-permute-done((f32[40,64]{1,0:T(8,128)S(1)}, f32[40,64]{1,0:T(8,128)S(1)}, u32[]{:S(2)}, u32[]{:S(2)}) %collective-permute-start.2) | collective-permute-done | bytes 10272 | tf_op jit(solution)/shard_map/ppermute | solution.py:49
  65.8 4.5 %collective-permute-done.3 = f32[40,64]{1,0:T(8,128)S(1)} collective-permute-done((f32[40,64]{1,0:T(8,128)S(1)}, f32[40,64]{1,0:T(8,128)S(1)}, u32[]{:S(2)}, u32[]{:S(2)}) %collective-permute-start.3) | collective-permute-done | bytes 10272 | tf_op jit(solution)/shard_map/ppermute | solution.py:49
  70.9 13.4 %collective-permute-start.23 = (bf16[2,4,352,128]{3,2,1,0:T(8,128)(2,1)S(1)}, bf16[2,4,352,128]{3,2,1,0:T(8,128)(2,1)S(1)}, u32[]{:S(2)}, u32[]{:S(2)}) collective-permute-start(bf16[2,4,352,128]{3,2,1,0:T(8,128)(2,1)S(1)} %get-tuple-element.31.refs_9_.refs_1_), channel_id=1, source_target_pairs={{0,224},{1,225},{2,226},{3,227},{4,228},{5,229},{6,230},{7,231},{8... | collective-permute-start | bytes 2162696 | tf_op jit(solution)/shard_map/ppermute | solution.py:49
  84.4 1.8 collective-permute-start.22
  86.2 6.4 %collective-permute-done.23.refs_11_.refs_3_ = bf16[2,4,352,128]{3,2,1,0:T(8,128)(2,1)S(1)} collective-permute-done((bf16[2,4,352,128]{3,2,1,0:T(8,128)(2,1)S(1)}, bf16[2,4,352,128]{3,2,1,0:T(8,128)(2,1)S(1)}, u32[]{:S(2)}, u32[]{:S(2)}) %collective-permute-start.23) | collective-permute-done | bytes 720928 | tf_op jit(solution)/shard_map/ppermute | solution.py:49
  94.3 6.3 %collective-permute-done.22.refs_10_.refs_2_ = bf16[2,4,352,128]{3,2,1,0:T(8,128)(2,1)} collective-permute-done((bf16[2,4,352,128]{3,2,1,0:T(8,128)(2,1)S(1)}, bf16[2,4,352,128]{3,2,1,0:T(8,128)(2,1)}, u32[]{:S(2)}, u32[]{:S(2)}) %collective-permute-start.22) | collective-permute-done | bytes 720928 | tf_op jit(solution)/shard_map/ppermute | solution.py:49
  101.5 3.5 %collective-permute-start.15 = (bf16[2,4,704,128]{3,2,1,0:T(8,128)(2,1)S(1)}, bf16[2,4,704,128]{3,2,1,0:T(8,128)(2,1)}, u32[]{:S(2)}, u32[]{:S(2)}) collective-permute-start(bf16[2,4,704,128]{3,2,1,0:T(8,128)(2,1)S(1)} %shard_map.138.refs_0_), channel_id=1, source_target_pairs={{0,2},{1,9},{2,4},{3,11},{4,6},{5,13},{6,0},{7,15},{8,10},{9,17},{... | collective-permute-start | bytes 4325384 | tf_op jit(solution)/shard_map/ppermute | solution.py:49
  105.0 1.5 collective-permute-start.14
  106.4 1.2 collective-permute-start.12
  108.5 3.4 %collective-permute-start.24 = (bf16[2,4,352,128]{3,2,1,0:T(8,128)(2,1)}, bf16[2,4,352,128]{3,2,1,0:T(8,128)(2,1)}, u32[]{:S(2)}, u32[]{:S(2)}) collective-permute-start(bf16[2,4,352,128]{3,2,1,0:T(8,128)(2,1)} %collective-permute-done.22.refs_10_.refs_2_), channel_id=1, source_target_pairs={{0,224},{1,225},{2,226},{3,227},{4,228},{5,229},{6,230},{7,231},{8... | collective-permute-start | bytes 2162696 | tf_op jit(solution)/shard_map/ppermute | solution.py:49
  112.0 1.0 pad_maximum_fusion
  113.8 10.0 %collective-permute-done.24.refs_12_.refs_4_ = bf16[2,4,352,128]{3,2,1,0:T(8,128)(2,1)} collective-permute-done((bf16[2,4,352,128]{3,2,1,0:T(8,128)(2,1)}, bf16[2,4,352,128]{3,2,1,0:T(8,128)(2,1)}, u32[]{:S(2)}, u32[]{:S(2)}) %collective-permute-start.24) | collective-permute-done | bytes 720928 | tf_op jit(solution)/shard_map/ppermute | solution.py:49
  123.7 3.1 %collective-permute-start.32 = (bf16[4,4,160,128]{3,2,1,0:T(8,128)(2,1)S(1)}, bf16[4,4,160,128]{3,2,1,0:T(8,128)(2,1)S(1)}, u32[]{:S(2)}, u32[]{:S(2)}) collective-permute-start(bf16[4,4,160,128]{3,2,1,0:T(8,128)(2,1)S(1)} %get-tuple-element.36.refs_4_.refs_0_), channel_id=1, source_target_pairs={{0,224},{1,225},{2,226},{3,227},{4,228},{5,229},{6,230},{7,231},{8... | collective-permute-start | bytes 1966088 | tf_op jit(solution)/shard_map/ppermute | solution.py:49
  126.9 1.9 maximum_select_fusion.x_ref.base_ref
  129.1 7.4 %collective-permute-done.14.refs_5_ = bf16[2,4,704,128]{3,2,1,0:T(8,128)(2,1)} collective-permute-done((bf16[2,4,704,128]{3,2,1,0:T(8,128)(2,1)}, bf16[2,4,704,128]{3,2,1,0:T(8,128)(2,1)}, u32[]{:S(2)}, u32[]{:S(2)}) %collective-permute-start.14) | collective-permute-done | bytes 1441824 | tf_op jit(solution)/shard_map/ppermute | solution.py:49
  136.5 4.0 %collective-permute-start.30 = (bf16[4,4,352,128]{3,2,1,0:T(8,128)(2,1)}, bf16[4,4,352,128]{3,2,1,0:T(8,128)(2,1)S(1)}, u32[]{:S(2)}, u32[]{:S(2)}) collective-permute-start(bf16[4,4,352,128]{3,2,1,0:T(8,128)(2,1)} %copy-done.9), channel_id=1, source_target_pairs={{0,4},{1,17},{2,6},{3,19},{4,0},{5,21},{6,2},{7,23},{8,12},{9,25},... | collective-permute-start | bytes 4325384 | tf_op jit(solution)/shard_map/ppermute | solution.py:49
  140.5 1.1 copy-done.7
  141.6 13.0 %shard_map.143 = (bf16[256,2048]{1,0:T(8,128)(2,1)S(1)}, bf16[4,4,4,704,128]{4,3,2,1,0:T(8,128)(2,1)S(1)}) custom-call(s32[3]{0:T(128)S(1)} %pad_add_fusion.place_ref, bf16[256,2048]{1,0:T(8,128)(2,1)S(1)} %maximum_select_fusion.x_ref.base_ref, bf16[2,4,704,128]{3,2,1,0:T(8,128)(2,1)S(1)} %shard_map.138.refs_0_, ...), custom_call_target="tpu_custom_call" | custom-call | flops 4400000000 | bytes 1000000 | tf_op jit(solution)/shard_map/pallas_call | solution.py:375
  154.6 19.0 %collective-permute-start.28 = (bf16[256,2048]{1,0:T(8,128)(2,1)S(1)}, bf16[256,2048]{1,0:T(8,128)(2,1)S(1)}, u32[]{:S(2)}, u32[]{:S(2)}) collective-permute-start(bf16[256,2048]{1,0:T(8,128)(2,1)S(1)} %get-tuple-element.32.mine_ref), channel_id=1, source_target_pairs={{0,1},{1,0},{2,3},{3,2},{4,5},{5,4},{6,7},{7,6},{8,9},{9,8},{10,11... | collective-permute-start | bytes 3145736 | tf_op jit(solution)/shard_map/ppermute | solution.py:406
  173.6 3.6 %collective-permute-start.34 = (bf16[4,4,160,128]{3,2,1,0:T(8,128)(2,1)S(1)}, bf16[4,4,160,128]{3,2,1,0:T(8,128)(2,1)S(1)}, u32[]{:S(2)}, u32[]{:S(2)}) collective-permute-start(bf16[4,4,160,128]{3,2,1,0:T(8,128)(2,1)S(1)} %get-tuple-element.36.refs_4_.refs_0_), channel_id=1, source_target_pairs={{0,32},{1,33},{2,34},{3,35},{4,36},{5,37},{6,38},{7,39},{8,40},{9,... | collective-permute-start | bytes 1966088 | tf_op jit(solution)/shard_map/ppermute | solution.py:49
  177.2 14.9 %collective-permute-done.34.refs_7_.refs_3_ = bf16[4,4,160,128]{3,2,1,0:T(8,128)(2,1)S(1)} collective-permute-done((bf16[4,4,160,128]{3,2,1,0:T(8,128)(2,1)S(1)}, bf16[4,4,160,128]{3,2,1,0:T(8,128)(2,1)S(1)}, u32[]{:S(2)}, u32[]{:S(2)}) %collective-permute-start.34) | collective-permute-done | bytes 655392 | tf_op jit(solution)/shard_map/ppermute | solution.py:49
  192.2 7.1 %shard_map.144 = (bf16[256,2048]{1,0:T(8,128)(2,1)S(1)}, bf16[256,256]{1,0:T(8,128)(2,1)S(1)}, bf16[256,256]{1,0:T(8,128)(2,1)S(1)}, bf16[256,512]{1,0:T(8,128)(...) custom-call(s32[3]{0:T(128)S(1)} %pad_add_fusion.place_ref, ...), custom_call_target="tpu_custom_call" | custom-call | flops 2000000000 | bytes 1000000 | tf_op jit(solution)/shard_map/pallas_call | solution.py:375
  199.3 4.7 %collective-permute-start.35 = (f32[136,256]{1,0:T(8,128)S(1)}, f32[136,256]{1,0:T(8,128)S(1)}, u32[]{:S(2)}, u32[]{:S(2)}) collective-permute-start(f32[136,256]{1,0:T(8,128)S(1)} %get-tuple-element.44), channel_id=1, source_target_pairs={{0,2},{2,4},{4,6},{1,3},{3,5},{5,7},{8,10},{10,12},{12,14},{9,11},... | collective-permute-start | bytes 417800 | tf_op jit(solution)/shard_map/ppermute | solution.py:472
  204.0 2.8 %collective-permute-start.36 = (f32[136,256]{1,0:T(8,128)S(1)}, f32[136,256]{1,0:T(8,128)S(1)}, u32[]{:S(2)}, u32[]{:S(2)}) collective-permute-start(f32[136,256]{1,0:T(8,128)S(1)} %get-tuple-element.44), channel_id=1, source_target_pairs={{0,4},{2,6},{1,5},{3,7},{8,12},{10,14},{9,13},{11,15},{16,20},{18,... | collective-permute-start | bytes 417800 | tf_op jit(solution)/shard_map/ppermute | solution.py:472
  206.8 1.3 collective-permute-start.37
  208.1 5.6 %shard_map.145.mixed_ref = f32[256,512]{1,0:T(8,128)S(1)} custom-call(bf16[256,256]{1,0:T(8,128)(2,1)S(1)} %get-tuple-element.38.q_ref, bf16[256,256]{1,0:T(8,128)(2,1)S(1)} %get-tuple-element.39.k_ref, bf16[256,512]{1,0:T(8,128)(2,1)S(1)} %get-tuple-element.40.v_ref, bf16[256,256]{1,0:T(8,128)(2,1)S(1)} %get-tuple-element.41.ghi_ref, ...), custom_call_target="tpu_custom_call" | custom-call | flops 4000000000 | bytes 1000000 | tf_op jit(solution)/shard_map/pallas_call | solution.py:375
  213.8 2.7 %shard_map.146.mine_ref = bf16[256,2048]{1,0:T(8,128)(2,1)S(1)} custom-call(s32[3]{0:T(128)S(1)} %pad_add_fusion.place_ref, f32[256,512]{1,0:T(8,128)S(1)} %shard_map.145.mixed_ref, bf16[256,256]{1,0:T(8,128)(2,1)S(1)} %get-tuple-element.38.q_ref, bf16[256,256]{1,0:T(8,128)(2,1)S(1)} %get-tuple-element.41.ghi_ref, ...), custom_call_target="tpu_custom_call" | custom-call | flops 1000000000 | bytes 1000000 | tf_op jit(solution)/shard_map/pallas_call | solution.py:375
  216.5 1.4 collective-permute-start.38
  217.9 2.3 collective-permute-done.38.other_ref
  220.2 10.0 %shard_map.147 = (bf16[128,2048]{1,0:T(8,128)(2,1)S(1)}, bf16[128,2048]{1,0:T(8,128)(2,1)S(1)}, bf16[128,2048]{1,0:T(8,128)(2,1)S(1)}) custom-call(s32[3]{0:T(128)S(1)} %pad_add_fusion.place_ref, bf16[256,2048]{1,0:T(8,128)(2,1)S(1)} %get-tuple-element.37.base_ref, bf16[256,2048]{1,0:T(8,128)(2,1)S(1)} %shard_map.146.mine_ref, ...), custom_call_target="tpu_custom_call" | custom-call | flops 4400000000 | bytes 1000000 | tf_op jit(solution)/shard_map/pallas_call | solution.py:375
  230.7 1.5 collective-permute-done.39.other_ref
  232.3 1.4 shard_map.148
  (98 shorter events, 8.9 us)
Async XLA Ops:
  1.2 9.9 %collective-permute-start.4 = (bf16[1056,128]{1,0:T(8,128)(2,1)S(1)}, bf16[1056,128]{1,0:T(8,128)(2,1)S(1)}, u32[]{:S(2)}, u32[]{:S(2)}) collective-permute-start(bf16[1056,128]{1,0:T(8,128)(2,1)S(1)} %get-tuple-element.28.refs_0_), channel_id=1, source_target_pairs={{0,224},{1,7},{2,226},{3,1},{4,228},{5,3},{6,230},{7,5},{8,232},{9... | collective-permute-start | bytes 811016 | tf_op jit(solution)/shard_map/ppermute | solution.py:49
  4.8 7.5 %collective-permute-start.5 = (bf16[1056,128]{1,0:T(8,128)(2,1)S(1)}, bf16[1056,128]{1,0:T(8,128)(2,1)S(1)}, u32[]{:S(2)}, u32[]{:S(2)}) collective-permute-start(bf16[1056,128]{1,0:T(8,128)(2,1)S(1)} %get-tuple-element.28.refs_0_), channel_id=1, source_target_pairs={{0,192},{1,5},{2,194},{3,7},{4,196},{5,1},{6,198},{7,3},{8,200},{9... | collective-permute-start | bytes 811016 | tf_op jit(solution)/shard_map/ppermute | solution.py:49
  5.2 9.7 %collective-permute-start.6 = (bf16[1056,128]{1,0:T(8,128)(2,1)S(1)}, bf16[1056,128]{1,0:T(8,128)(2,1)S(1)}, u32[]{:S(2)}, u32[]{:S(2)}) collective-permute-start(bf16[1056,128]{1,0:T(8,128)(2,1)S(1)} %get-tuple-element.28.refs_0_), channel_id=1, source_target_pairs={{0,32},{1,3},{2,34},{3,5},{4,36},{5,7},{6,38},{7,1},{8,40},{9,11},... | collective-permute-start | bytes 811016 | tf_op jit(solution)/shard_map/ppermute | solution.py:49
  5.9 15.9 %collective-permute-start.16 = (bf16[512,128]{1,0:T(8,128)(2,1)S(1)}, bf16[512,128]{1,0:T(8,128)(2,1)S(1)}, u32[]{:S(2)}, u32[]{:S(2)}) collective-permute-start(bf16[512,128]{1,0:T(8,128)(2,1)S(1)} %get-tuple-element.30.refs_0_), channel_id=1, source_target_pairs={{0,24},{1,25},{2,26},{3,27},{4,28},{5,29},{6,30},{7,31},{8,0},{9,1... | collective-permute-start | bytes 393224 | tf_op jit(solution)/shard_map/ppermute | solution.py:49
  8.3 13.4 %collective-permute-start.17 = (bf16[512,128]{1,0:T(8,128)(2,1)S(1)}, bf16[512,128]{1,0:T(8,128)(2,1)S(1)}, u32[]{:S(2)}, u32[]{:S(2)}) collective-permute-start(bf16[512,128]{1,0:T(8,128)(2,1)S(1)} %get-tuple-element.30.refs_0_), channel_id=1, source_target_pairs={{0,16},{1,17},{2,18},{3,19},{4,20},{5,21},{6,22},{7,23},{8,24},{9,... | collective-permute-start | bytes 393224 | tf_op jit(solution)/shard_map/ppermute | solution.py:49
  11.1 10.6 %collective-permute-start.18 = (bf16[512,128]{1,0:T(8,128)(2,1)S(1)}, bf16[512,128]{1,0:T(8,128)(2,1)S(1)}, u32[]{:S(2)}, u32[]{:S(2)}) collective-permute-start(bf16[512,128]{1,0:T(8,128)(2,1)S(1)} %get-tuple-element.30.refs_0_), channel_id=1, source_target_pairs={{0,8},{1,9},{2,10},{3,11},{4,12},{5,13},{6,14},{7,15},{8,16},{9,17... | collective-permute-start | bytes 393224 | tf_op jit(solution)/shard_map/ppermute | solution.py:49
  14.9 35.7 %collective-permute-start.7 = (bf16[4,1056,128]{2,1,0:T(8,128)(2,1)S(1)}, bf16[4,1056,128]{2,1,0:T(8,128)(2,1)S(1)}, u32[]{:S(2)}, u32[]{:S(2)}) collective-permute-start(bf16[4,1056,128]{2,1,0:T(8,128)(2,1)S(1)} %shard_map.137.plane.refs_0_), channel_id=1, source_target_pairs={{0,24},{1,225},{2,26},{3,227},{4,28},{5,229},{6,30},{7,231},{8,0},... | collective-permute-start | bytes 3244040 | tf_op jit(solution)/shard_map/ppermute | solution.py:49
  20.3 30.3 %collective-permute-start.8 = (bf16[4,1056,128]{2,1,0:T(8,128)(2,1)S(1)}, bf16[4,1056,128]{2,1,0:T(8,128)(2,1)S(1)}, u32[]{:S(2)}, u32[]{:S(2)}) collective-permute-start(bf16[4,1056,128]{2,1,0:T(8,128)(2,1)S(1)} %shard_map.137.plane.refs_0_), channel_id=1, source_target_pairs={{0,16},{1,193},{2,18},{3,195},{4,20},{5,197},{6,22},{7,199},{8,24}... | collective-permute-start | bytes 3244040 | tf_op jit(solution)/shard_map/ppermute | solution.py:49
  21.7 28.9 %collective-permute-start.9 = (bf16[4,1056,128]{2,1,0:T(8,128)(2,1)S(1)}, bf16[4,1056,128]{2,1,0:T(8,128)(2,1)S(1)}, u32[]{:S(2)}, u32[]{:S(2)}) collective-permute-start(bf16[4,1056,128]{2,1,0:T(8,128)(2,1)S(1)} %shard_map.137.plane.refs_0_), channel_id=1, source_target_pairs={{0,8},{1,33},{2,10},{3,35},{4,12},{5,37},{6,14},{7,39},{8,16},{9,4... | collective-permute-start | bytes 3244040 | tf_op jit(solution)/shard_map/ppermute | solution.py:49
  21.8 13.0 %collective-permute-start.19 = (bf16[4,512,128]{2,1,0:T(8,128)(2,1)S(1)}, bf16[4,512,128]{2,1,0:T(8,128)(2,1)S(1)}, u32[]{:S(2)}, u32[]{:S(2)}) collective-permute-start(bf16[4,512,128]{2,1,0:T(8,128)(2,1)S(1)} %shard_map.140.plane.refs_0_), channel_id=1, source_target_pairs={{0,6},{1,7},{2,0},{3,1},{4,2},{5,3},{6,4},{7,5},{8,14},{9,15},{10,... | collective-permute-start | bytes 1572872 | tf_op jit(solution)/shard_map/ppermute | solution.py:49
  22.8 12.3 %collective-permute-start.20 = (bf16[4,512,128]{2,1,0:T(8,128)(2,1)S(1)}, bf16[4,512,128]{2,1,0:T(8,128)(2,1)S(1)}, u32[]{:S(2)}, u32[]{:S(2)}) collective-permute-start(bf16[4,512,128]{2,1,0:T(8,128)(2,1)S(1)} %shard_map.140.plane.refs_0_), channel_id=1, source_target_pairs={{0,4},{1,5},{2,6},{3,7},{4,0},{5,1},{6,2},{7,3},{8,12},{9,13},{10,... | collective-permute-start | bytes 1572872 | tf_op jit(solution)/shard_map/ppermute | solution.py:49
  34.8 12.5 %collective-permute-start.21 = (bf16[4,512,128]{2,1,0:T(8,128)(2,1)S(1)}, bf16[4,512,128]{2,1,0:T(8,128)(2,1)S(1)}, u32[]{:S(2)}, u32[]{:S(2)}) collective-permute-start(bf16[4,512,128]{2,1,0:T(8,128)(2,1)S(1)} %shard_map.140.plane.refs_0_), channel_id=1, source_target_pairs={{0,2},{1,3},{2,4},{3,5},{4,6},{5,7},{6,0},{7,1},{8,10},{9,11},{10,... | collective-permute-start | bytes 1572872 | tf_op jit(solution)/shard_map/ppermute | solution.py:49
  47.3 38.9 %collective-permute-start.25 = (bf16[2,4,352,128]{3,2,1,0:T(8,128)(2,1)S(1)}, bf16[2,4,352,128]{3,2,1,0:T(8,128)(2,1)S(1)}, u32[]{:S(2)}, u32[]{:S(2)}) collective-permute-start(bf16[2,4,352,128]{3,2,1,0:T(8,128)(2,1)S(1)} %get-tuple-element.31.refs_9_.refs_1_), channel_id=1, source_target_pairs={{0,32},{1,33},{2,34},{3,35},{4,36},{5,37},{6,38},{7,39},{8,40},{9,... | collective-permute-start | bytes 2162696 | tf_op jit(solution)/shard_map/ppermute | solution.py:49
  51.9 53.0 %collective-permute-start.13 = (bf16[2,4,704,128]{3,2,1,0:T(8,128)(2,1)}, bf16[2,4,704,128]{3,2,1,0:T(8,128)(2,1)}, u32[]{:S(2)}, u32[]{:S(2)}) collective-permute-start(bf16[2,4,704,128]{3,2,1,0:T(8,128)(2,1)} %get-tuple-element.29.refs_1_), channel_id=1, source_target_pairs={{0,2},{1,9},{2,4},{3,11},{4,6},{5,13},{6,0},{7,15},{8,10},{9,17},{... | collective-permute-start | bytes 4325384 | tf_op jit(solution)/shard_map/ppermute | solution.py:49
  53.0 53.4 %collective-permute-start.10 = (bf16[2,4,704,128]{3,2,1,0:T(8,128)(2,1)S(1)}, bf16[2,4,704,128]{3,2,1,0:T(8,128)(2,1)}, u32[]{:S(2)}, u32[]{:S(2)}) collective-permute-start(bf16[2,4,704,128]{3,2,1,0:T(8,128)(2,1)S(1)} %shard_map.138.refs_0_), channel_id=1, source_target_pairs={{0,6},{1,25},{2,0},{3,27},{4,2},{5,29},{6,4},{7,31},{8,14},{9,1},{... | collective-permute-start | bytes 4325384 | tf_op jit(solution)/shard_map/ppermute | solution.py:49
  57.5 26.9 %collective-permute-start = (bf16[128,2048]{1,0:T(8,128)(2,1)S(1)}, bf16[128,2048]{1,0:T(8,128)(2,1)S(1)}, u32[]{:S(2)}, u32[]{:S(2)}) collective-permute-start(bf16[128,2048]{1,0:T(8,128)(2,1)S(1)} %copy-done.13), channel_id=1, source_target_pairs={{0,1},{1,0},{2,3},{3,2},{4,5},{5,4},{6,7},{7,6},{8,9},{9,8},{10,11... | collective-permute-start | bytes 1572872 | tf_op jit(solution)/shard_map/ppermute | solution.py:406
  58.1 3.3 %collective-permute-start.1 = (f32[40,64]{1,0:T(8,128)S(1)}, f32[40,64]{1,0:T(8,128)S(1)}, u32[]{:S(2)}, u32[]{:S(2)}) collective-permute-start(f32[40,64]{1,0:T(8,128)S(1)} %pad_maximum_fusion.1), channel_id=1, source_target_pairs={{0,6},{1,7},{2,0},{3,1},{4,2},{5,3},{6,4},{7,5},{8,14},{9,15},{10,... | collective-permute-start | bytes 30728 | tf_op jit(solution)/shard_map/ppermute | solution.py:49
  61.5 8.8 %copy-start.15 = (f32[40,64]{1,0:T(8,128)}, f32[40,64]{1,0:T(8,128)S(1)}, u32[]{:S(2)}) copy-start(f32[40,64]{1,0:T(8,128)S(1)} %collective-permute-done.1) | copy-start | bytes 30724
  61.5 4.4 %collective-permute-start.2 = (f32[40,64]{1,0:T(8,128)S(1)}, f32[40,64]{1,0:T(8,128)S(1)}, u32[]{:S(2)}, u32[]{:S(2)}) collective-permute-start(f32[40,64]{1,0:T(8,128)S(1)} %pad_maximum_fusion.1), channel_id=1, source_target_pairs={{0,4},{1,5},{2,6},{3,7},{4,0},{5,1},{6,2},{7,3},{8,12},{9,13},{10,... | collective-permute-start | bytes 30728 | tf_op jit(solution)/shard_map/ppermute | solution.py:49
  65.8 4.5 %collective-permute-start.3 = (f32[40,64]{1,0:T(8,128)S(1)}, f32[40,64]{1,0:T(8,128)S(1)}, u32[]{:S(2)}, u32[]{:S(2)}) collective-permute-start(f32[40,64]{1,0:T(8,128)S(1)} %pad_maximum_fusion.1), channel_id=1, source_target_pairs={{0,2},{1,3},{2,4},{3,5},{4,6},{5,7},{6,0},{7,1},{8,10},{9,11},{10,... | collective-permute-start | bytes 30728 | tf_op jit(solution)/shard_map/ppermute | solution.py:49
  70.9 21.7 %collective-permute-start.23 = (bf16[2,4,352,128]{3,2,1,0:T(8,128)(2,1)S(1)}, bf16[2,4,352,128]{3,2,1,0:T(8,128)(2,1)S(1)}, u32[]{:S(2)}, u32[]{:S(2)}) collective-permute-start(bf16[2,4,352,128]{3,2,1,0:T(8,128)(2,1)S(1)} %get-tuple-element.31.refs_9_.refs_1_), channel_id=1, source_target_pairs={{0,224},{1,225},{2,226},{3,227},{4,228},{5,229},{6,230},{7,231},{8... | collective-permute-start | bytes 2162696 | tf_op jit(solution)/shard_map/ppermute | solution.py:49
  84.4 23.2 %copy-start.14 = (bf16[128,2048]{1,0:T(8,128)(2,1)}, bf16[128,2048]{1,0:T(8,128)(2,1)S(1)}, u32[]{:S(2)}) copy-start(bf16[128,2048]{1,0:T(8,128)(2,1)S(1)} %collective-permute-done) | copy-start | bytes 1572868
  84.4 16.2 %collective-permute-start.22 = (bf16[2,4,352,128]{3,2,1,0:T(8,128)(2,1)S(1)}, bf16[2,4,352,128]{3,2,1,0:T(8,128)(2,1)}, u32[]{:S(2)}, u32[]{:S(2)}) collective-permute-start(bf16[2,4,352,128]{3,2,1,0:T(8,128)(2,1)S(1)} %shard_map.141.refs_8_.refs_0_), channel_id=1, source_target_pairs={{0,224},{1,225},{2,226},{3,227},{4,228},{5,229},{6,230},{7,231},{8... | collective-permute-start | bytes 2162696 | tf_op jit(solution)/shard_map/ppermute | solution.py:49
  86.2 14.4 %collective-permute-start.27 = (bf16[2,4,352,128]{3,2,1,0:T(8,128)(2,1)S(1)}, bf16[2,4,352,128]{3,2,1,0:T(8,128)(2,1)S(1)}, u32[]{:S(2)}, u32[]{:S(2)}) collective-permute-start(bf16[2,4,352,128]{3,2,1,0:T(8,128)(2,1)S(1)} %shard_map.141.refs_8_.refs_0_), channel_id=1, source_target_pairs={{0,32},{1,33},{2,34},{3,35},{4,36},{5,37},{6,38},{7,39},{8,40},{9,... | collective-permute-start | bytes 2162696 | tf_op jit(solution)/shard_map/ppermute | solution.py:49
  93.4 14.2 %collective-permute-start.26 = (bf16[2,4,352,128]{3,2,1,0:T(8,128)(2,1)S(1)}, bf16[2,4,352,128]{3,2,1,0:T(8,128)(2,1)S(1)}, u32[]{:S(2)}, u32[]{:S(2)}) collective-permute-start(bf16[2,4,352,128]{3,2,1,0:T(8,128)(2,1)S(1)} %collective-permute-done.25.refs_15_.refs_7_), channel_id=1, source_target_pairs={{0,32},{1,33},{2,34},{3,35},{4,36},{5,37},{6,38},{7,39},{8,40},{9,... | collective-permute-start | bytes 2162696 | tf_op jit(solution)/shard_map/ppermute | solution.py:49
  100.6 28.2 %collective-permute-start.11 = (bf16[2,4,704,128]{3,2,1,0:T(8,128)(2,1)}, bf16[2,4,704,128]{3,2,1,0:T(8,128)(2,1)}, u32[]{:S(2)}, u32[]{:S(2)}) collective-permute-start(bf16[2,4,704,128]{3,2,1,0:T(8,128)(2,1)} %get-tuple-element.29.refs_1_), channel_id=1, source_target_pairs={{0,6},{1,25},{2,0},{3,27},{4,2},{5,29},{6,4},{7,31},{8,14},{9,1},{... | collective-permute-start | bytes 4325384 | tf_op jit(solution)/shard_map/ppermute | solution.py:49
  101.5 27.6 %collective-permute-start.15 = (bf16[2,4,704,128]{3,2,1,0:T(8,128)(2,1)S(1)}, bf16[2,4,704,128]{3,2,1,0:T(8,128)(2,1)}, u32[]{:S(2)}, u32[]{:S(2)}) collective-permute-start(bf16[2,4,704,128]{3,2,1,0:T(8,128)(2,1)S(1)} %shard_map.138.refs_0_), channel_id=1, source_target_pairs={{0,2},{1,9},{2,4},{3,11},{4,6},{5,13},{6,0},{7,15},{8,10},{9,17},{... | collective-permute-start | bytes 4325384 | tf_op jit(solution)/shard_map/ppermute | solution.py:49
  105.0 31.5 %collective-permute-start.14 = (bf16[2,4,704,128]{3,2,1,0:T(8,128)(2,1)}, bf16[2,4,704,128]{3,2,1,0:T(8,128)(2,1)}, u32[]{:S(2)}, u32[]{:S(2)}) collective-permute-start(bf16[2,4,704,128]{3,2,1,0:T(8,128)(2,1)} %collective-permute-done.13.refs_7_), channel_id=1, source_target_pairs={{0,2},{1,9},{2,4},{3,11},{4,6},{5,13},{6,0},{7,15},{8,10},{9,17},{... | collective-permute-start | bytes 4325384 | tf_op jit(solution)/shard_map/ppermute | solution.py:49
  106.4 34.0 %collective-permute-start.12 = (bf16[2,4,704,128]{3,2,1,0:T(8,128)(2,1)}, bf16[2,4,704,128]{3,2,1,0:T(8,128)(2,1)}, u32[]{:S(2)}, u32[]{:S(2)}) collective-permute-start(bf16[2,4,704,128]{3,2,1,0:T(8,128)(2,1)} %collective-permute-done.10.refs_2_), channel_id=1, source_target_pairs={{0,6},{1,25},{2,0},{3,27},{4,2},{5,29},{6,4},{7,31},{8,14},{9,1},{... | collective-permute-start | bytes 4325384 | tf_op jit(solution)/shard_map/ppermute | solution.py:49
  108.5 15.2 %collective-permute-start.24 = (bf16[2,4,352,128]{3,2,1,0:T(8,128)(2,1)}, bf16[2,4,352,128]{3,2,1,0:T(8,128)(2,1)}, u32[]{:S(2)}, u32[]{:S(2)}) collective-permute-start(bf16[2,4,352,128]{3,2,1,0:T(8,128)(2,1)} %collective-permute-done.22.refs_10_.refs_2_), channel_id=1, source_target_pairs={{0,224},{1,225},{2,226},{3,227},{4,228},{5,229},{6,230},{7,231},{8... | collective-permute-start | bytes 2162696 | tf_op jit(solution)/shard_map/ppermute | solution.py:49
  111.9 28.5 %copy-start.1 = (bf16[2,4,352,128]{3,2,1,0:T(8,128)(2,1)S(1)}, bf16[2,4,352,128]{3,2,1,0:T(8,128)(2,1)}, u32[]{:S(2)}) copy-start(bf16[2,4,352,128]{3,2,1,0:T(8,128)(2,1)} %copy-done) | copy-start | bytes 2162692
  111.9 28.6 %copy-start.3 = (bf16[2,4,352,128]{3,2,1,0:T(8,128)(2,1)S(1)}, bf16[2,4,352,128]{3,2,1,0:T(8,128)(2,1)}, u32[]{:S(2)}) copy-start(bf16[2,4,352,128]{3,2,1,0:T(8,128)(2,1)} %copy-done.2) | copy-start | bytes 2162692
  111.9 28.6 %copy-start.5 = (bf16[2,4,352,128]{3,2,1,0:T(8,128)(2,1)S(1)}, bf16[2,4,352,128]{3,2,1,0:T(8,128)(2,1)}, u32[]{:S(2)}) copy-start(bf16[2,4,352,128]{3,2,1,0:T(8,128)(2,1)} %copy-done.4) | copy-start | bytes 2162692
  123.7 30.8 %collective-permute-start.32 = (bf16[4,4,160,128]{3,2,1,0:T(8,128)(2,1)S(1)}, bf16[4,4,160,128]{3,2,1,0:T(8,128)(2,1)S(1)}, u32[]{:S(2)}, u32[]{:S(2)}) collective-permute-start(bf16[4,4,160,128]{3,2,1,0:T(8,128)(2,1)S(1)} %get-tuple-element.36.refs_4_.refs_0_), channel_id=1, source_target_pairs={{0,224},{1,225},{2,226},{3,227},{4,228},{5,229},{6,230},{7,231},{8... | collective-permute-start | bytes 1966088 | tf_op jit(solution)/shard_map/ppermute | solution.py:49
  128.8 44.8 %collective-permute-start.33 = (bf16[4,4,160,128]{3,2,1,0:T(8,128)(2,1)S(1)}, bf16[4,4,160,128]{3,2,1,0:T(8,128)(2,1)S(1)}, u32[]{:S(2)}, u32[]{:S(2)}) collective-permute-start(bf16[4,4,160,128]{3,2,1,0:T(8,128)(2,1)S(1)} %get-tuple-element.36.refs_4_.refs_0_), channel_id=1, source_target_pairs={{0,192},{1,193},{2,194},{3,195},{4,196},{5,197},{6,198},{7,199},{8... | collective-permute-start | bytes 1966088 | tf_op jit(solution)/shard_map/ppermute | solution.py:49
  129.1 63.0 %collective-permute-start.29 = (bf16[4,4,352,128]{3,2,1,0:T(8,128)(2,1)}, bf16[4,4,352,128]{3,2,1,0:T(8,128)(2,1)S(1)}, u32[]{:S(2)}, u32[]{:S(2)}) collective-permute-start(bf16[4,4,352,128]{3,2,1,0:T(8,128)(2,1)} %copy-done.9), channel_id=1, source_target_pairs={{0,6},{1,25},{2,0},{3,27},{4,2},{5,29},{6,4},{7,31},{8,14},{9,1},{... | collective-permute-start | bytes 4325384 | tf_op jit(solution)/shard_map/ppermute | solution.py:49
  136.5 55.7 %collective-permute-start.30 = (bf16[4,4,352,128]{3,2,1,0:T(8,128)(2,1)}, bf16[4,4,352,128]{3,2,1,0:T(8,128)(2,1)S(1)}, u32[]{:S(2)}, u32[]{:S(2)}) collective-permute-start(bf16[4,4,352,128]{3,2,1,0:T(8,128)(2,1)} %copy-done.9), channel_id=1, source_target_pairs={{0,4},{1,17},{2,6},{3,19},{4,0},{5,21},{6,2},{7,23},{8,12},{9,25},... | collective-permute-start | bytes 4325384 | tf_op jit(solution)/shard_map/ppermute | solution.py:49
  140.4 51.7 %collective-permute-start.31 = (bf16[4,4,352,128]{3,2,1,0:T(8,128)(2,1)}, bf16[4,4,352,128]{3,2,1,0:T(8,128)(2,1)S(1)}, u32[]{:S(2)}, u32[]{:S(2)}) collective-permute-start(bf16[4,4,352,128]{3,2,1,0:T(8,128)(2,1)} %copy-done.9), channel_id=1, source_target_pairs={{0,2},{1,9},{2,4},{3,11},{4,6},{5,13},{6,0},{7,15},{8,10},{9,17},{... | collective-permute-start | bytes 4325384 | tf_op jit(solution)/shard_map/ppermute | solution.py:49
  141.6 35.6 %copy-start.19 = (f32[3,2048]{1,0:T(4,128)S(1)}, f32[3,2048]{1,0:T(4,128)}, u32[]{:S(2)}) copy-start(f32[3,2048]{1,0:T(4,128)} %param.27) | copy-start | bytes 73732
  141.6 50.5 %copy-start.10 = (bf16[4,4,352,128]{3,2,1,0:T(8,128)(2,1)S(1)}, bf16[4,4,352,128]{3,2,1,0:T(8,128)(2,1)}, u32[]{:S(2)}) copy-start(bf16[4,4,352,128]{3,2,1,0:T(8,128)(2,1)} %copy-done.9) | copy-start | bytes 4325380
  141.6 50.6 %copy-start.11 = (bf16[2048,32]{0,1:T(8,128)(2,1)S(1)}, bf16[2048,32]{0,1:T(8,128)(2,1)}, u32[]{:S(2)}) copy-start(bf16[2048,32]{0,1:T(8,128)(2,1)} %param.22) | copy-start | bytes 393220
  154.6 37.6 %collective-permute-start.28 = (bf16[256,2048]{1,0:T(8,128)(2,1)S(1)}, bf16[256,2048]{1,0:T(8,128)(2,1)S(1)}, u32[]{:S(2)}, u32[]{:S(2)}) collective-permute-start(bf16[256,2048]{1,0:T(8,128)(2,1)S(1)} %get-tuple-element.32.mine_ref), channel_id=1, source_target_pairs={{0,1},{1,0},{2,3},{3,2},{4,5},{5,4},{6,7},{7,6},{8,9},{9,8},{10,11... | collective-permute-start | bytes 3145736 | tf_op jit(solution)/shard_map/ppermute | solution.py:406
  173.6 18.5 %collective-permute-start.34 = (bf16[4,4,160,128]{3,2,1,0:T(8,128)(2,1)S(1)}, bf16[4,4,160,128]{3,2,1,0:T(8,128)(2,1)S(1)}, u32[]{:S(2)}, u32[]{:S(2)}) collective-permute-start(bf16[4,4,160,128]{3,2,1,0:T(8,128)(2,1)S(1)} %get-tuple-element.36.refs_4_.refs_0_), channel_id=1, source_target_pairs={{0,32},{1,33},{2,34},{3,35},{4,36},{5,37},{6,38},{7,39},{8,40},{9,... | collective-permute-start | bytes 1966088 | tf_op jit(solution)/shard_map/ppermute | solution.py:49
  199.3 14.5 %collective-permute-start.35 = (f32[136,256]{1,0:T(8,128)S(1)}, f32[136,256]{1,0:T(8,128)S(1)}, u32[]{:S(2)}, u32[]{:S(2)}) collective-permute-start(f32[136,256]{1,0:T(8,128)S(1)} %get-tuple-element.44), channel_id=1, source_target_pairs={{0,2},{2,4},{4,6},{1,3},{3,5},{5,7},{8,10},{10,12},{12,14},{9,11},... | collective-permute-start | bytes 417800 | tf_op jit(solution)/shard_map/ppermute | solution.py:472
  204.0 9.8 %collective-permute-start.36 = (f32[136,256]{1,0:T(8,128)S(1)}, f32[136,256]{1,0:T(8,128)S(1)}, u32[]{:S(2)}, u32[]{:S(2)}) collective-permute-start(f32[136,256]{1,0:T(8,128)S(1)} %get-tuple-element.44), channel_id=1, source_target_pairs={{0,4},{2,6},{1,5},{3,7},{8,12},{10,14},{9,13},{11,15},{16,20},{18,... | collective-permute-start | bytes 417800 | tf_op jit(solution)/shard_map/ppermute | solution.py:472
  206.8 6.9 %collective-permute-start.37 = (f32[136,256]{1,0:T(8,128)S(1)}, f32[136,256]{1,0:T(8,128)S(1)}, u32[]{:S(2)}, u32[]{:S(2)}) collective-permute-start(f32[136,256]{1,0:T(8,128)S(1)} %get-tuple-element.44), channel_id=1, source_target_pairs={{0,6},{1,7},{8,14},{9,15},{16,22},{17,23},{24,30},{25,31},{32,38},... | collective-permute-start | bytes 417800 | tf_op jit(solution)/shard_map/ppermute | solution.py:472
  216.5 3.7 %collective-permute-start.38 = (bf16[256,2048]{1,0:T(8,128)(2,1)S(1)}, bf16[256,2048]{1,0:T(8,128)(2,1)S(1)}, u32[]{:S(2)}, u32[]{:S(2)}) collective-permute-start(bf16[256,2048]{1,0:T(8,128)(2,1)S(1)} %shard_map.146.mine_ref), channel_id=1, source_target_pairs={{0,1},{1,0},{2,3},{3,2},{4,5},{5,4},{6,7},{7,6},{8,9},{9,8},{10,11... | collective-permute-start | bytes 3145736 | tf_op jit(solution)/shard_map/ppermute | solution.py:406
  230.3 2.0 collective-permute-start.39
  (14 other events, 40.9 us)
where the time goes:
time: 235 us; the launch traced here: 234 us
  starting transfers between devices  91 us (39%)
  waiting for transfers between devices  90 us (38%)
  Pallas kernels  42.6 us (18%)
  local copies, waits for them, and re-layouts  5.97 us (3%)
  other arithmetic  3.75 us (2%)
    ppermute x33, waiting for transfers between devices, shifted(): return lax.ppermute(value, tuple(AXES), pairs)  86.2 us
    ppermute x33, starting transfers between devices, shifted(): return lax.ppermute(value, tuple(AXES), pairs)  61.2 us
    pallas_call x13, Pallas kernels, call(): pl.pallas_call(kernel, out_shape=[jax.ShapeDtypeStruct(*out) for out in o...  42.6 us
    ppermute x4, starting transfers between devices, swapped(): return lax.ppermute(value, 'c', [(0, 1), (1, 0)])  20.9 us
    ppermute x3, starting transfers between devices, on_device(): lax.ppermute(state, 'y', [(i, i + back) for i in range(4 - back)])  8.84 us
    unnamed x44, local copies, waits for them, and re-layouts  5.94 us
  transfers between devices with their start and end apart: 40, of which 15 were waited for; matrix products, arithmetic and copies ran while one was open for 2% of the time, Pallas kernels for 9%

commit v1 on v0

--- a/solution.py
+++ b/solution.py
@@ -26,8 +26,10 @@
 
 F32 = jnp.float32
 BF16 = jnp.bfloat16
-LARGE = ("zxy", "yzx")
-SMALL = ("xyz", "xyz")
+LARGE = ("yxz", "zyx")
+SMALL = ("xzy", "xzy")
+NEAR = (0, 1, 3)
+FAR = (2,)
 AXES = {"r": 2, "z": 4, "x": 4, "y": 4, "c": 2}
 VMEM_LIMIT = 20 * 1024 * 1024
 
@@ -96,16 +98,22 @@
     return lax.dot_general(a, b, (((1,), (1,)), ((), ())), preferred_element_type=F32)
 
 
-def ordered_columns(place_ref, ref):
+def block_offsets(place_ref, i, j):
+    core = place_ref[2]
+    return i + core * (j - i), j + core * (i - j)
+
+
+def ordered_columns(place_ref, ref, outer):
     blocks = []
-    for dx in range(4):
-        for dz in range(4):
-            blocks.append(ref[:, pl.ds(pl.multiple_of(fs_block(place_ref, dz, dx) * LANE, LANE), LANE)])
+    for i in outer:
+        for j in range(4):
+            column = fs_block(place_ref, *block_offsets(place_ref, i, j)) * LANE
+            blocks.append(ref[:, pl.ds(pl.multiple_of(column, LANE), LANE)])
     return jnp.concatenate(blocks, axis=1)
 
 
-def joined_features(block):
-    return jnp.concatenate([block(dx, dz) for dx in range(4) for dz in range(4)], axis=1)
+def joined_features(block, outer):
+    return jnp.concatenate([block(i, j) for i in outer for j in range(4)], axis=1)
 
 
 def prepare_kernel(gate_ref, up_ref, query_ref, key_ref, value_ref, outgate_ref, down_ref, out_ref, *refs):
@@ -147,33 +155,27 @@
         mix[n] = plane[:, units:]
 
 
-def arranged(place_ref, pieces, halves, y, dst):
+def arranged(place_ref, piece, y, dst):
+    halves = len(piece)
     inner = 4 // halves
-    for k in range(4):
-
-        @pl.when((place_ref[2] == 0) & (y == k))
+    for half, ref in enumerate(piece):
+
+        @pl.when(place_ref[2] == 0)
         def _():
-            for half in range(halves):
-
-                @pl.loop(0, inner)
-                def _(n):
-                    for dz in range(4):
-                        dst[half * inner + n, dz] = pieces[halves * k + half][n, dz]
-
-    @pl.when(place_ref[2] == 1)
-    def _():
-        for dx in range(4):
-            for half in range(halves):
-
-                @pl.loop(0, inner)
-                def _(n):
-                    dst[dx, half * inner + n] = pieces[halves * dx + half][n, y]
-
-
-def hidden_units(x, large, y, hidden):
-    both = dot_t(x, joined_features(lambda dx, dz: large[y, dx, dz]))
+            @pl.loop(0, inner)
+            def _(n):
+                dst[half * inner + n] = ref[n, y]
+
+        @pl.when((place_ref[2] == 1) & (y >= half * inner) & (y < (half + 1) * inner))
+        def _():
+            @pl.loop(0, 4)
+            def _(n):
+                dst[n] = ref[y - half * inner, n]
+
+
+def gated_units(both):
     gate, upward = both[:, :HID], both[:, HID:]
-    hidden[y] = (gate / (1.0 + jnp.exp(-gate)) * upward).astype(BF16)
+    return (gate / (1.0 + jnp.exp(-gate)) * upward).astype(BF16)
 
 
 def projected(place_ref, units, block, store):
@@ -186,15 +188,26 @@
             store(pl.ds(column, LANE), part[:, dz * LANE : (dz + 1) * LANE])
 
 
-def ffn_first_kernel(place_ref, x_ref, *refs):
-    large_p, small_p = refs[:8], refs[8:16]
-    out_ref, large_ref, hidden = refs[16:]
-    x = ordered_columns(place_ref, x_ref)
+def ffn_early_kernel(place_ref, x_ref, *refs):
+    near_ref, part_ref = refs[6:]
+    x = ordered_columns(place_ref, x_ref, NEAR)
 
     @pl.loop(0, 4)
     def _(y):
-        arranged(place_ref, large_p, 2, y, large_ref.at[y])
-        hidden_units(x, large_ref, y, hidden)
+        for n in range(3):
+            arranged(place_ref, refs[2 * n : 2 * n + 2], y, near_ref.at[y, n])
+        part_ref[y] = dot_t(x, joined_features(lambda n, j: near_ref[y, n, j], range(3)))
+
+
+def ffn_late_kernel(place_ref, x_ref, part_ref, *refs):
+    small_p = refs[2:10]
+    out_ref, far_ref, hidden = refs[10:]
+    x = ordered_columns(place_ref, x_ref, FAR)
+
+    @pl.loop(0, 4)
+    def _(y):
+        arranged(place_ref, refs[:2], y, far_ref.at[y])
+        hidden[y] = gated_units(part_ref[y] + dot_t(x, joined_features(lambda i, j: far_ref[y, j], FAR)))
 
     def store(columns, value):
         out_ref[:, columns] = value
@@ -202,22 +215,23 @@
     projected(
         place_ref,
         lambda: jnp.concatenate([hidden[y] for y in range(4)], axis=1),
-        lambda dz, y, dx: small_p[2 * dz + y // 2][y % 2, dx],
+        lambda dz, y, dx: small_p[2 * y + dz // 2][dz % 2, dx],
         store,
     )
 
 
-def ffn_second_kernel(place_ref, base_ref, mine_ref, other_ref, gain_ref, large_ref, *refs):
+def ffn_second_kernel(place_ref, base_ref, mine_ref, other_ref, gain_ref, near_ref, far_ref, *refs):
     small_p = refs[:8]
     own_ref, keep_ref, give_ref, hidden, second = refs[8:]
     core = place_ref[2]
     after_branch(second, base_ref, mine_ref, other_ref, gain_ref, 1.0)
     own_ref[...] = second[pl.ds(pl.multiple_of(core * 128, 128), 128), :]
-    x = ordered_columns(place_ref, second)
+    x = ordered_columns(place_ref, second, NEAR + FAR)
 
     @pl.loop(0, 4)
     def _(y):
-        hidden_units(x, large_ref, y, hidden)
+        rows = joined_features(lambda n, j: far_ref[y, j] if n == 3 else near_ref[y, n, j], range(4))
+        hidden[y] = gated_units(dot_t(x, rows))
 
     def store(columns, value):
         keep_ref[:, columns] = jnp.where(core == 0, value[:128], value[128:])
@@ -226,7 +240,7 @@
     projected(
         place_ref,
         lambda: jnp.concatenate([hidden[y] for y in range(4)], axis=1),
-        lambda dz, y, dx: small_p[2 * dz + y // 2][y % 2, dx],
+        lambda dz, y, dx: small_p[2 * y + dz // 2][dz % 2, dx],
         store,
     )
 
@@ -250,7 +264,7 @@
 
 
 def project_kernel(place_ref, base_ref, mine_ref, other_ref, gain_ref, down_ref, up_ref, bias_ref, *refs):
-    first_ref, q_ref, k_ref, v_ref, outgate_ref, ghi_ref, glo_ref, state_ref, parts, large = refs[8:]
+    first_ref, q_ref, k_ref, v_ref, outgate_ref, ghi_ref, glo_ref, state_ref, parts, large, tails = refs[8:]
     large_p, small_p = refs[:4], refs[4:8]
     after_branch(first_ref, base_ref, mine_ref, other_ref, gain_ref, BRANCH_SCALE)
     first = first_ref[...]
@@ -261,14 +275,24 @@
     glo = (log_gate - ghi.astype(F32)).astype(BF16)
     ghi_ref[...] = ghi
     glo_ref[...] = glo
-    x = ordered_columns(place_ref, first_ref)
+    x = ordered_columns(place_ref, first_ref, range(4))
 
     @pl.loop(0, 4)
     def _(y):
-        arranged(place_ref, large_p, 1, y, large)
+        for n in range(4):
+            arranged(place_ref, large_p[n : n + 1], y, large.at[n])
+
+            @pl.when(y == n)
+            def _():
+                @pl.loop(0, 4)
+                def _(i):
+                    for j in range(4):
+                        dz, dx = block_offsets(place_ref, i, j)
+                        tails[i, j] = small_p[n][dz, dx, :TAIL]
+
         rows = [
-            joined_features(lambda dx, dz: large[dx, dz]),
-            joined_features(lambda dx, dz: small_p[dz][y, dx, :TAIL]),
+            joined_features(lambda i, j: large[i, j], range(4)),
+            joined_features(lambda i, j: tails[i, j], range(4)),
         ]
         parts[y] = dot_t(x, jnp.concatenate(rows, axis=0)).astype(BF16)
 
@@ -363,7 +387,7 @@
     def store(columns, value):
         out_ref[:, columns] = value
 
-    projected(place_ref, lambda: channels, lambda dz, y, dx: refs[dz][y, dx, TAIL:], store)
+    projected(place_ref, lambda: channels, lambda dz, y, dx: refs[y][dz, dx, TAIL:], store)
 
 
 def call(kernel, outs, scalars, arrays, scratch=(), flops=1_000_000, space=pltpu.VMEM):
@@ -441,13 +465,22 @@
     decay = jnp.concatenate([decay, *shifts], axis=1)
 
     rows, decay_rows, decay_bias_row = lax.optimization_barrier((rows, decay[:32].astype(BF16), decay[32:33]))
-    part, large = call(
-        ffn_first_kernel,
-        [((ROWS, D), BF16), ((4, 4, 4, 2 * HID, LANE), BF16)],
+    large_p, small_p = flat_ffn[:8], flat_ffn[8:]
+    near, part = call(
+        ffn_early_kernel,
+        [((4, 3, 4, 2 * HID, LANE), BF16), ((4, ROWS, 2 * HID), F32)],
         [place],
-        [rows, *flat_ffn],
+        [rows, *large_p[:4], *large_p[6:]],
+        (),
+        2_200_000_000,
+    )
+    part, far = call(
+        ffn_late_kernel,
+        [((ROWS, D), BF16), ((4, 4, 2 * HID, LANE), BF16)],
+        [place],
+        [rows, part, *large_p[4:6], *small_p],
         FFN_SCRATCH,
-        4_400_000_000,
+        2_200_000_000,
     )
     wide = ((ROWS, HEADS * DK), BF16)
     broad = ((ROWS, HEADS * DV), BF16)
@@ -465,7 +498,7 @@
             decay_bias_row,
             *flat_mix,
         ],
-        [pltpu.VMEM((4, ROWS, MIX + TAIL), BF16), pltpu.VMEM((4, 4, MIX, LANE), BF16)],
+        [pltpu.VMEM((4, ROWS, MIX + TAIL), BF16), pltpu.VMEM((4, 4, MIX, LANE), BF16), pltpu.VMEM((4, 4, TAIL, LANE), BF16)],
         2_000_000_000,
     )
     earlier = [
@@ -491,7 +524,7 @@
         ffn_second_kernel,
         [((128, D), BF16)] * 3,
         [place],
-        [first, part, swapped(part), norm_gain[1:2], large, *flat_ffn[8:]],
+        [first, part, swapped(part), norm_gain[1:2], near, far, *small_p],
         [*FFN_SCRATCH, pltpu.VMEM((ROWS, D), BF16)],
         4_400_000_000,
     )

time: 235 us -> 222 us (0.945)
  starting transfers between devices: 91 us -> 68.3 us
  waiting for transfers between devices: 90 us -> 97.7 us
  Pallas kernels: 42.6 us -> 45.6 us
    ppermute x33, starting transfers between devices: 61.2 us -> 44.8 us  [shifted(): return lax.ppermute(value, tuple(AXES), pairs)]
    ppermute x33, waiting for transfers between devices: 86.2 us -> 93.9 us  [shifted(): return lax.ppermute(value, tuple(AXES), pairs)]
    ppermute x4, starting transfers between devices: 20.9 us -> 15.7 us  [swapped(): return lax.ppermute(value, 'c', [(0, 1), (1, 0)])]
    pallas_call x13 -> x14, Pallas kernels: 42.6 us -> 45.6 us  [call(): pl.pallas_call(kernel, out_shape=[jax.ShapeDtypeStruct(*out) for out in o...]
    unnamed x44 -> x42, local copies, waits for them, and re-layouts: 5.94 us -> 5.7 us
  transfers between devices with their start and end apart: 40 -> 40, of which waited for: 15 -> 15; matrix products, arithmetic and copies ran while one was open for 2% -> 2% of each run, Pallas kernels for 9% -> 10%
where the time goes in v1:
time: 222 us; the launch traced here: 221 us
  waiting for transfers between devices  97.7 us (44%)
  starting transfers between devices  68.3 us (31%)
  Pallas kernels  45.6 us (21%)
  local copies, waits for them, and re-layouts  5.73 us (3%)
  other arithmetic  3.71 us (2%)
    ppermute x33, waiting for transfers between devices, shifted(): return lax.ppermute(value, tuple(AXES), pairs)  93.9 us
    pallas_call x14, Pallas kernels, call(): pl.pallas_call(kernel, out_shape=[jax.ShapeDtypeStruct(*out) for out in o...  45.6 us
    ppermute x33, starting transfers between devices, shifted(): return lax.ppermute(value, tuple(AXES), pairs)  44.8 us
    ppermute x4, starting transfers between devices, swapped(): return lax.ppermute(value, 'c', [(0, 1), (1, 0)])  15.7 us
    ppermute x3, starting transfers between devices, on_device(): lax.ppermute(state, 'y', [(i, i + back) for i in range(4 - back)])  7.76 us
    unnamed x42, local copies, waits for them, and re-layouts  5.7 us
  transfers between devices with their start and end apart: 40, of which 15 were waited for; matrix products, arithmetic and copies ran while one was open for 2% of the time, Pallas kernels for 10%

profile of v1, /device:TPU:1, one launch (start us, length us, event | category | flops | bytes accessed | tf_op | source)
XLA Modules:
  0.0 221.4 jit_solution(10021257511236639870)
XLA Ops:
  0.0 1.2 shard_map.136
  1.2 6.5 %collective-permute-start.4 = (bf16[1056,128]{1,0:T(8,128)(2,1)S(1)}, bf16[1056,128]{1,0:T(8,128)(2,1)S(1)}, u32[]{:S(2)}, u32[]{:S(2)}) collective-permute-start(bf16[1056,128]{1,0:T(8,128)(2,1)S(1)} %get-tuple-element.30.refs_0_), channel_id=1, source_target_pairs={{0,6},{1,225},{2,0},{3,227},{4,2},{5,229},{6,4},{7,231},{8,14},{9,... | collective-permute-start | bytes 811016 | tf_op jit(solution)/shard_map/ppermute | solution.py:51
  7.7 1.2 collective-permute-start.5
  8.8 2.5 %collective-permute-start.16 = (bf16[512,128]{1,0:T(8,128)(2,1)S(1)}, bf16[512,128]{1,0:T(8,128)(2,1)S(1)}, u32[]{:S(2)}, u32[]{:S(2)}) collective-permute-start(bf16[512,128]{1,0:T(8,128)(2,1)S(1)} %get-tuple-element.33.refs_0_), channel_id=1, source_target_pairs={{0,24},{1,25},{2,26},{3,27},{4,28},{5,29},{6,30},{7,31},{8,0},{9,1... | collective-permute-start | bytes 393224 | tf_op jit(solution)/shard_map/ppermute | solution.py:51
  12.5 1.7 collective-permute-done.5.refs_2_
  14.2 1.5 collective-permute-done.6.refs_3_
  15.7 2.6 %collective-permute-start.7 = (bf16[4,1056,128]{2,1,0:T(8,128)(2,1)S(1)}, bf16[4,1056,128]{2,1,0:T(8,128)(2,1)S(1)}, u32[]{:S(2)}, u32[]{:S(2)}) collective-permute-start(bf16[4,1056,128]{2,1,0:T(8,128)(2,1)S(1)} %shard_map.137.plane.refs_0_), channel_id=1, source_target_pairs={{0,24},{1,7},{2,26},{3,1},{4,28},{5,3},{6,30},{7,5},{8,0},{9,15},{... | collective-permute-start | bytes 3244040 | tf_op jit(solution)/shard_map/ppermute | solution.py:51
  20.4 1.4 collective-permute-start.19
  21.8 1.6 collective-permute-start.20
  23.3 10.0 %collective-permute-done.19.ahead.refs_1_ = bf16[4,512,128]{2,1,0:T(8,128)(2,1)S(1)} collective-permute-done((bf16[4,512,128]{2,1,0:T(8,128)(2,1)S(1)}, bf16[4,512,128]{2,1,0:T(8,128)(2,1)S(1)}, u32[]{:S(2)}, u32[]{:S(2)}) %collective-permute-start.19) | collective-permute-done | bytes 524320 | tf_op jit(solution)/shard_map/ppermute | solution.py:51
  33.4 1.3 collective-permute-start.21
  34.6 11.0 %collective-permute-done.20.refs_2_ = bf16[4,512,128]{2,1,0:T(8,128)(2,1)S(1)} collective-permute-done((bf16[4,512,128]{2,1,0:T(8,128)(2,1)S(1)}, bf16[4,512,128]{2,1,0:T(8,128)(2,1)S(1)}, u32[]{:S(2)}, u32[]{:S(2)}) %collective-permute-start.20) | collective-permute-done | bytes 524320 | tf_op jit(solution)/shard_map/ppermute | solution.py:51
  45.7 2.3 %collective-permute-start.25 = (bf16[2,4,352,128]{3,2,1,0:T(8,128)(2,1)S(1)}, bf16[2,4,352,128]{3,2,1,0:T(8,128)(2,1)S(1)}, u32[]{:S(2)}, u32[]{:S(2)}) collective-permute-start(bf16[2,4,352,128]{3,2,1,0:T(8,128)(2,1)S(1)} %get-tuple-element.34.refs_3_.refs_1_), channel_id=1, source_target_pairs={{0,2},{1,3},{2,4},{3,5},{4,6},{5,7},{6,0},{7,1},{8,10},{9,11},{10,... | collective-permute-start | bytes 2162696 | tf_op jit(solution)/shard_map/ppermute | solution.py:51
  48.0 1.3 shard_map.139
  50.5 1.8 collective-permute-start.10
  52.3 6.0 %collective-permute-start = (bf16[128,2048]{1,0:T(8,128)(2,1)S(1)}, bf16[128,2048]{1,0:T(8,128)(2,1)S(1)}, u32[]{:S(2)}, u32[]{:S(2)}) collective-permute-start(bf16[128,2048]{1,0:T(8,128)(2,1)S(1)} %copy-done.12), channel_id=1, source_target_pairs={{0,1},{1,0},{2,3},{3,2},{4,5},{5,4},{6,7},{7,6},{8,9},{9,8},{10,11... | collective-permute-start | bytes 1572872 | tf_op jit(solution)/shard_map/ppermute | solution.py:430
  58.9 3.0 %collective-permute-start.1 = (f32[40,64]{1,0:T(8,128)S(1)}, f32[40,64]{1,0:T(8,128)S(1)}, u32[]{:S(2)}, u32[]{:S(2)}) collective-permute-start(f32[40,64]{1,0:T(8,128)S(1)} %pad_maximum_fusion.1), channel_id=1, source_target_pairs={{0,6},{1,7},{2,0},{3,1},{4,2},{5,3},{6,4},{7,5},{8,14},{9,15},{10,... | collective-permute-start | bytes 30728 | tf_op jit(solution)/shard_map/ppermute | solution.py:51
  62.8 1.8 collective-permute-start.2
  64.7 2.5 %collective-permute-done.2 = f32[40,64]{1,0:T(8,128)S(1)} collective-permute-done((f32[40,64]{1,0:T(8,128)S(1)}, f32[40,64]{1,0:T(8,128)S(1)}, u32[]{:S(2)}, u32[]{:S(2)}) %collective-permute-start.2) | collective-permute-done | bytes 10272 | tf_op jit(solution)/shard_map/ppermute | solution.py:51
  67.2 1.1 collective-permute-start.3
  68.3 3.6 %collective-permute-done.3 = f32[40,64]{1,0:T(8,128)S(1)} collective-permute-done((f32[40,64]{1,0:T(8,128)S(1)}, f32[40,64]{1,0:T(8,128)S(1)}, u32[]{:S(2)}, u32[]{:S(2)}) %collective-permute-start.3) | collective-permute-done | bytes 10272 | tf_op jit(solution)/shard_map/ppermute | solution.py:51
  72.5 1.5 collective-permute-start.23
  74.1 1.4 collective-permute-start.27
  75.6 12.2 %collective-permute-done.23.refs_5_.refs_3_ = bf16[2,4,352,128]{3,2,1,0:T(8,128)(2,1)S(1)} collective-permute-done((bf16[2,4,352,128]{3,2,1,0:T(8,128)(2,1)S(1)}, bf16[2,4,352,128]{3,2,1,0:T(8,128)(2,1)S(1)}, u32[]{:S(2)}, u32[]{:S(2)}) %collective-permute-start.23) | collective-permute-done | bytes 720928 | tf_op jit(solution)/shard_map/ppermute | solution.py:51
  89.5 13.8 %collective-permute-done.22.refs_4_.refs_2_ = bf16[2,4,352,128]{3,2,1,0:T(8,128)(2,1)} collective-permute-done((bf16[2,4,352,128]{3,2,1,0:T(8,128)(2,1)S(1)}, bf16[2,4,352,128]{3,2,1,0:T(8,128)(2,1)}, u32[]{:S(2)}, u32[]{:S(2)}) %collective-permute-start.22) | collective-permute-done | bytes 720928 | tf_op jit(solution)/shard_map/ppermute | solution.py:51
  104.2 1.5 collective-permute-start.12
  105.7 2.7 %collective-permute-start.14 = (bf16[2,4,704,128]{3,2,1,0:T(8,128)(2,1)}, bf16[2,4,704,128]{3,2,1,0:T(8,128)(2,1)}, u32[]{:S(2)}, u32[]{:S(2)}) collective-permute-start(bf16[2,4,704,128]{3,2,1,0:T(8,128)(2,1)} %collective-permute-done.10.refs_2_), channel_id=1, source_target_pairs={{0,224},{1,25},{2,226},{3,27},{4,228},{5,29},{6,230},{7,31},{8,232... | collective-permute-start | bytes 4325384 | tf_op jit(solution)/shard_map/ppermute | solution.py:51
  109.2 2.4 %collective-permute-start.24 = (bf16[2,4,352,128]{3,2,1,0:T(8,128)(2,1)}, bf16[2,4,352,128]{3,2,1,0:T(8,128)(2,1)}, u32[]{:S(2)}, u32[]{:S(2)}) collective-permute-start(bf16[2,4,352,128]{3,2,1,0:T(8,128)(2,1)} %collective-permute-done.22.refs_4_.refs_2_), channel_id=1, source_target_pairs={{0,6},{1,7},{2,0},{3,1},{4,2},{5,3},{6,4},{7,5},{8,14},{9,15},{10,... | collective-permute-start | bytes 2162696 | tf_op jit(solution)/shard_map/ppermute | solution.py:51
  113.4 9.4 %collective-permute-done.24.refs_6_.refs_4_ = bf16[2,4,352,128]{3,2,1,0:T(8,128)(2,1)} collective-permute-done((bf16[2,4,352,128]{3,2,1,0:T(8,128)(2,1)}, bf16[2,4,352,128]{3,2,1,0:T(8,128)(2,1)}, u32[]{:S(2)}, u32[]{:S(2)}) %collective-permute-start.24) | collective-permute-done | bytes 720928 | tf_op jit(solution)/shard_map/ppermute | solution.py:51
  122.9 3.3 %collective-permute-start.32 = (bf16[4,4,160,128]{3,2,1,0:T(8,128)(2,1)S(1)}, bf16[4,4,160,128]{3,2,1,0:T(8,128)(2,1)S(1)}, u32[]{:S(2)}, u32[]{:S(2)}) collective-permute-start(bf16[4,4,160,128]{3,2,1,0:T(8,128)(2,1)S(1)} %get-tuple-element.39.refs_4_.refs_0_), channel_id=1, source_target_pairs={{0,6},{1,7},{2,0},{3,1},{4,2},{5,3},{6,4},{7,5},{8,14},{9,15},{10,... | collective-permute-start | bytes 1966088 | tf_op jit(solution)/shard_map/ppermute | solution.py:51
  126.1 1.9 maximum_select_fusion.x_ref.base_ref
  128.2 1.4 collective-permute-start.29
  129.6 9.5 %collective-permute-done.15.refs_1_ = bf16[2,4,704,128]{3,2,1,0:T(8,128)(2,1)} collective-permute-done((bf16[2,4,704,128]{3,2,1,0:T(8,128)(2,1)}, bf16[2,4,704,128]{3,2,1,0:T(8,128)(2,1)}, u32[]{:S(2)}, u32[]{:S(2)}) %collective-permute-start.15) | collective-permute-done | bytes 1441824 | tf_op jit(solution)/shard_map/ppermute | solution.py:51
  139.7 7.8 %shard_map.140 = (bf16[4,3,4,704,128]{4,3,2,1,0:T(8,128)(2,1)S(1)}, f32[4,256,704]{2,1,0:T(8,128)S(1)}) custom-call(s32[3]{0:T(128)S(1)} %pad_add_fusion.place_ref, bf16[256,2048]{1,0:T(8,128)(2,1)S(1)} %maximum_select_fusion.x_ref.base_ref, bf16[2,4,704,128]{3,2,1,0:T(8,128)(2,1)S(1)} %shard_map.138.refs_0_, ...), custom_call_target="tpu_custom_call" | custom-call | flops 2200000000 | bytes 1000000 | tf_op jit(solution)/shard_map/pallas_call | solution.py:399
  147.5 7.5 %shard_map.144 = (bf16[256,2048]{1,0:T(8,128)(2,1)S(1)}, bf16[4,4,704,128]{3,2,1,0:T(8,128)(2,1)S(1)}) custom-call(s32[3]{0:T(128)S(1)} %pad_add_fusion.place_ref, bf16[256,2048]{1,0:T(8,128)(2,1)S(1)} %maximum_select_fusion.x_ref.base_ref, f32[4,256,704]{2,1,0:T(8,128)S(1)} %get-tuple-element.32.part_ref, ...), custom_call_target="tpu_custom_call" | custom-call | flops 2200000000 | bytes 1000000 | tf_op jit(solution)/shard_map/pallas_call | solution.py:399
  155.0 7.7 %collective-permute-start.28 = (bf16[256,2048]{1,0:T(8,128)(2,1)S(1)}, bf16[256,2048]{1,0:T(8,128)(2,1)S(1)}, u32[]{:S(2)}, u32[]{:S(2)}) collective-permute-start(bf16[256,2048]{1,0:T(8,128)(2,1)S(1)} %get-tuple-element.35.mine_ref), channel_id=1, source_target_pairs={{0,1},{1,0},{2,3},{3,2},{4,5},{5,4},{6,7},{7,6},{8,9},{9,8},{10,11... | collective-permute-start | bytes 3145736 | tf_op jit(solution)/shard_map/ppermute | solution.py:430
  163.2 16.9 %collective-permute-done.34.refs_7_.refs_3_ = bf16[4,4,160,128]{3,2,1,0:T(8,128)(2,1)S(1)} collective-permute-done((bf16[4,4,160,128]{3,2,1,0:T(8,128)(2,1)S(1)}, bf16[4,4,160,128]{3,2,1,0:T(8,128)(2,1)S(1)}, u32[]{:S(2)}, u32[]{:S(2)}) %collective-permute-start.34) | collective-permute-done | bytes 655392 | tf_op jit(solution)/shard_map/ppermute | solution.py:51
  180.1 7.6 %shard_map.145 = (bf16[256,2048]{1,0:T(8,128)(2,1)S(1)}, bf16[256,256]{1,0:T(8,128)(2,1)S(1)}, bf16[256,256]{1,0:T(8,128)(2,1)S(1)}, bf16[256,512]{1,0:T(8,128)(...) custom-call(s32[3]{0:T(128)S(1)} %pad_add_fusion.place_ref, ...), custom_call_target="tpu_custom_call" | custom-call | flops 2000000000 | bytes 1000000 | tf_op jit(solution)/shard_map/pallas_call | solution.py:399
  187.8 1.3 collective-permute-start.35
  189.1 5.2 %collective-permute-start.36 = (f32[136,256]{1,0:T(8,128)S(1)}, f32[136,256]{1,0:T(8,128)S(1)}, u32[]{:S(2)}, u32[]{:S(2)}) collective-permute-start(f32[136,256]{1,0:T(8,128)S(1)} %get-tuple-element.47), channel_id=1, source_target_pairs={{0,4},{2,6},{1,5},{3,7},{8,12},{10,14},{9,13},{11,15},{16,20},{18,... | collective-permute-start | bytes 417800 | tf_op jit(solution)/shard_map/ppermute | solution.py:505
  194.3 1.3 collective-permute-start.37
  195.6 5.6 %shard_map.146.mixed_ref = f32[256,512]{1,0:T(8,128)S(1)} custom-call(bf16[256,256]{1,0:T(8,128)(2,1)S(1)} %get-tuple-element.41.q_ref, bf16[256,256]{1,0:T(8,128)(2,1)S(1)} %get-tuple-element.42.k_ref, bf16[256,512]{1,0:T(8,128)(2,1)S(1)} %get-tuple-element.43.v_ref, bf16[256,256]{1,0:T(8,128)(2,1)S(1)} %get-tuple-element.44.ghi_ref, ...), custom_call_target="tpu_custom_call" | custom-call | flops 4000000000 | bytes 1000000 | tf_op jit(solution)/shard_map/pallas_call | solution.py:399
  201.2 2.6 %shard_map.147.mine_ref = bf16[256,2048]{1,0:T(8,128)(2,1)S(1)} custom-call(s32[3]{0:T(128)S(1)} %pad_add_fusion.place_ref, f32[256,512]{1,0:T(8,128)S(1)} %shard_map.146.mixed_ref, bf16[256,256]{1,0:T(8,128)(2,1)S(1)} %get-tuple-element.41.q_ref, bf16[256,256]{1,0:T(8,128)(2,1)S(1)} %get-tuple-element.44.ghi_ref, ...), custom_call_target="tpu_custom_call" | custom-call | flops 1000000000 | bytes 1000000 | tf_op jit(solution)/shard_map/pallas_call | solution.py:399
  203.9 1.6 collective-permute-start.38
  205.5 2.3 %collective-permute-done.38.other_ref = bf16[256,2048]{1,0:T(8,128)(2,1)S(1)} collective-permute-done((bf16[256,2048]{1,0:T(8,128)(2,1)S(1)}, bf16[256,2048]{1,0:T(8,128)(2,1)S(1)}, u32[]{:S(2)}, u32[]{:S(2)}) %collective-permute-start.38) | collective-permute-done | bytes 1048608 | tf_op jit(solution)/shard_map/ppermute | solution.py:430
  207.8 10.2 %shard_map.148 = (bf16[128,2048]{1,0:T(8,128)(2,1)S(1)}, bf16[128,2048]{1,0:T(8,128)(2,1)S(1)}, bf16[128,2048]{1,0:T(8,128)(2,1)S(1)}) custom-call(s32[3]{0:T(128)S(1)} %pad_add_fusion.place_ref, bf16[256,2048]{1,0:T(8,128)(2,1)S(1)} %get-tuple-element.40.base_ref, bf16[256,2048]{1,0:T(8,128)(2,1)S(1)} %shard_map.147.mine_ref, ...), custom_call_target="tpu_custom_call" | custom-call | flops 4400000000 | bytes 1000000 | tf_op jit(solution)/shard_map/pallas_call | solution.py:399
  218.4 1.6 collective-permute-done.39.other_ref
  219.9 1.4 shard_map.149
  (97 shorter events, 13.8 us)
Async XLA Ops:
  1.2 10.6 %collective-permute-start.4 = (bf16[1056,128]{1,0:T(8,128)(2,1)S(1)}, bf16[1056,128]{1,0:T(8,128)(2,1)S(1)}, u32[]{:S(2)}, u32[]{:S(2)}) collective-permute-start(bf16[1056,128]{1,0:T(8,128)(2,1)S(1)} %get-tuple-element.30.refs_0_), channel_id=1, source_target_pairs={{0,6},{1,225},{2,0},{3,227},{4,2},{5,229},{6,4},{7,231},{8,14},{9,... | collective-permute-start | bytes 811016 | tf_op jit(solution)/shard_map/ppermute | solution.py:51
  7.7 6.5 %collective-permute-start.5 = (bf16[1056,128]{1,0:T(8,128)(2,1)S(1)}, bf16[1056,128]{1,0:T(8,128)(2,1)S(1)}, u32[]{:S(2)}, u32[]{:S(2)}) collective-permute-start(bf16[1056,128]{1,0:T(8,128)(2,1)S(1)} %get-tuple-element.30.refs_0_), channel_id=1, source_target_pairs={{0,4},{1,193},{2,6},{3,195},{4,0},{5,197},{6,2},{7,199},{8,12},{9,... | collective-permute-start | bytes 811016 | tf_op jit(solution)/shard_map/ppermute | solution.py:51
  8.8 6.8 %collective-permute-start.6 = (bf16[1056,128]{1,0:T(8,128)(2,1)S(1)}, bf16[1056,128]{1,0:T(8,128)(2,1)S(1)}, u32[]{:S(2)}, u32[]{:S(2)}) collective-permute-start(bf16[1056,128]{1,0:T(8,128)(2,1)S(1)} %get-tuple-element.30.refs_0_), channel_id=1, source_target_pairs={{0,2},{1,33},{2,4},{3,35},{4,6},{5,37},{6,0},{7,39},{8,10},{9,41},... | collective-permute-start | bytes 811016 | tf_op jit(solution)/shard_map/ppermute | solution.py:51
  8.8 10.1 %collective-permute-start.16 = (bf16[512,128]{1,0:T(8,128)(2,1)S(1)}, bf16[512,128]{1,0:T(8,128)(2,1)S(1)}, u32[]{:S(2)}, u32[]{:S(2)}) collective-permute-start(bf16[512,128]{1,0:T(8,128)(2,1)S(1)} %get-tuple-element.33.refs_0_), channel_id=1, source_target_pairs={{0,24},{1,25},{2,26},{3,27},{4,28},{5,29},{6,30},{7,31},{8,0},{9,1... | collective-permute-start | bytes 393224 | tf_op jit(solution)/shard_map/ppermute | solution.py:51
  11.3 8.3 %collective-permute-start.17 = (bf16[512,128]{1,0:T(8,128)(2,1)S(1)}, bf16[512,128]{1,0:T(8,128)(2,1)S(1)}, u32[]{:S(2)}, u32[]{:S(2)}) collective-permute-start(bf16[512,128]{1,0:T(8,128)(2,1)S(1)} %get-tuple-element.33.refs_0_), channel_id=1, source_target_pairs={{0,16},{1,17},{2,18},{3,19},{4,20},{5,21},{6,22},{7,23},{8,24},{9,... | collective-permute-start | bytes 393224 | tf_op jit(solution)/shard_map/ppermute | solution.py:51
  11.8 8.5 %collective-permute-start.18 = (bf16[512,128]{1,0:T(8,128)(2,1)S(1)}, bf16[512,128]{1,0:T(8,128)(2,1)S(1)}, u32[]{:S(2)}, u32[]{:S(2)}) collective-permute-start(bf16[512,128]{1,0:T(8,128)(2,1)S(1)} %get-tuple-element.33.refs_0_), channel_id=1, source_target_pairs={{0,8},{1,9},{2,10},{3,11},{4,12},{5,13},{6,14},{7,15},{8,16},{9,17... | collective-permute-start | bytes 393224 | tf_op jit(solution)/shard_map/ppermute | solution.py:51
  15.7 32.3 %collective-permute-start.7 = (bf16[4,1056,128]{2,1,0:T(8,128)(2,1)S(1)}, bf16[4,1056,128]{2,1,0:T(8,128)(2,1)S(1)}, u32[]{:S(2)}, u32[]{:S(2)}) collective-permute-start(bf16[4,1056,128]{2,1,0:T(8,128)(2,1)S(1)} %shard_map.137.plane.refs_0_), channel_id=1, source_target_pairs={{0,24},{1,7},{2,26},{3,1},{4,28},{5,3},{6,30},{7,5},{8,0},{9,15},{... | collective-permute-start | bytes 3244040 | tf_op jit(solution)/shard_map/ppermute | solution.py:51
  18.4 29.7 %collective-permute-start.8 = (bf16[4,1056,128]{2,1,0:T(8,128)(2,1)S(1)}, bf16[4,1056,128]{2,1,0:T(8,128)(2,1)S(1)}, u32[]{:S(2)}, u32[]{:S(2)}) collective-permute-start(bf16[4,1056,128]{2,1,0:T(8,128)(2,1)S(1)} %shard_map.137.plane.refs_0_), channel_id=1, source_target_pairs={{0,16},{1,5},{2,18},{3,7},{4,20},{5,1},{6,22},{7,3},{8,24},{9,13},... | collective-permute-start | bytes 3244040 | tf_op jit(solution)/shard_map/ppermute | solution.py:51
  18.9 29.1 %collective-permute-start.9 = (bf16[4,1056,128]{2,1,0:T(8,128)(2,1)S(1)}, bf16[4,1056,128]{2,1,0:T(8,128)(2,1)S(1)}, u32[]{:S(2)}, u32[]{:S(2)}) collective-permute-start(bf16[4,1056,128]{2,1,0:T(8,128)(2,1)S(1)} %shard_map.137.plane.refs_0_), channel_id=1, source_target_pairs={{0,8},{1,3},{2,10},{3,5},{4,12},{5,7},{6,14},{7,1},{8,16},{9,11},{... | collective-permute-start | bytes 3244040 | tf_op jit(solution)/shard_map/ppermute | solution.py:51
  20.4 13.0 %collective-permute-start.19 = (bf16[4,512,128]{2,1,0:T(8,128)(2,1)S(1)}, bf16[4,512,128]{2,1,0:T(8,128)(2,1)S(1)}, u32[]{:S(2)}, u32[]{:S(2)}) collective-permute-start(bf16[4,512,128]{2,1,0:T(8,128)(2,1)S(1)} %shard_map.141.plane.refs_0_), channel_id=1, source_target_pairs={{0,224},{1,225},{2,226},{3,227},{4,228},{5,229},{6,230},{7,231},{8... | collective-permute-start | bytes 1572872 | tf_op jit(solution)/shard_map/ppermute | solution.py:51
  21.8 23.8 %collective-permute-start.20 = (bf16[4,512,128]{2,1,0:T(8,128)(2,1)S(1)}, bf16[4,512,128]{2,1,0:T(8,128)(2,1)S(1)}, u32[]{:S(2)}, u32[]{:S(2)}) collective-permute-start(bf16[4,512,128]{2,1,0:T(8,128)(2,1)S(1)} %shard_map.141.plane.refs_0_), channel_id=1, source_target_pairs={{0,192},{1,193},{2,194},{3,195},{4,196},{5,197},{6,198},{7,199},{8... | collective-permute-start | bytes 1572872 | tf_op jit(solution)/shard_map/ppermute | solution.py:51
  33.4 12.2 %collective-permute-start.21 = (bf16[4,512,128]{2,1,0:T(8,128)(2,1)S(1)}, bf16[4,512,128]{2,1,0:T(8,128)(2,1)S(1)}, u32[]{:S(2)}, u32[]{:S(2)}) collective-permute-start(bf16[4,512,128]{2,1,0:T(8,128)(2,1)S(1)} %shard_map.141.plane.refs_0_), channel_id=1, source_target_pairs={{0,32},{1,33},{2,34},{3,35},{4,36},{5,37},{6,38},{7,39},{8,40},{9,... | collective-permute-start | bytes 1572872 | tf_op jit(solution)/shard_map/ppermute | solution.py:51
  45.7 28.4 %collective-permute-start.25 = (bf16[2,4,352,128]{3,2,1,0:T(8,128)(2,1)S(1)}, bf16[2,4,352,128]{3,2,1,0:T(8,128)(2,1)S(1)}, u32[]{:S(2)}, u32[]{:S(2)}) collective-permute-start(bf16[2,4,352,128]{3,2,1,0:T(8,128)(2,1)S(1)} %get-tuple-element.34.refs_3_.refs_1_), channel_id=1, source_target_pairs={{0,2},{1,3},{2,4},{3,5},{4,6},{5,7},{6,0},{7,1},{8,10},{9,11},{10,... | collective-permute-start | bytes 2162696 | tf_op jit(solution)/shard_map/ppermute | solution.py:51
  49.4 56.3 %collective-permute-start.13 = (bf16[2,4,704,128]{3,2,1,0:T(8,128)(2,1)}, bf16[2,4,704,128]{3,2,1,0:T(8,128)(2,1)}, u32[]{:S(2)}, u32[]{:S(2)}) collective-permute-start(bf16[2,4,704,128]{3,2,1,0:T(8,128)(2,1)} %get-tuple-element.31.refs_1_), channel_id=1, source_target_pairs={{0,32},{1,9},{2,34},{3,11},{4,36},{5,13},{6,38},{7,15},{8,40},{9,1... | collective-permute-start | bytes 4325384 | tf_op jit(solution)/shard_map/ppermute | solution.py:51
  50.5 55.2 %collective-permute-start.10 = (bf16[2,4,704,128]{3,2,1,0:T(8,128)(2,1)S(1)}, bf16[2,4,704,128]{3,2,1,0:T(8,128)(2,1)}, u32[]{:S(2)}, u32[]{:S(2)}) collective-permute-start(bf16[2,4,704,128]{3,2,1,0:T(8,128)(2,1)S(1)} %shard_map.138.refs_0_), channel_id=1, source_target_pairs={{0,224},{1,25},{2,226},{3,27},{4,228},{5,29},{6,230},{7,31},{8,232... | collective-permute-start | bytes 4325384 | tf_op jit(solution)/shard_map/ppermute | solution.py:51
  52.3 21.7 %collective-permute-start = (bf16[128,2048]{1,0:T(8,128)(2,1)S(1)}, bf16[128,2048]{1,0:T(8,128)(2,1)S(1)}, u32[]{:S(2)}, u32[]{:S(2)}) collective-permute-start(bf16[128,2048]{1,0:T(8,128)(2,1)S(1)} %copy-done.12), channel_id=1, source_target_pairs={{0,1},{1,0},{2,3},{3,2},{4,5},{5,4},{6,7},{7,6},{8,9},{9,8},{10,11... | collective-permute-start | bytes 1572872 | tf_op jit(solution)/shard_map/ppermute | solution.py:430
  58.9 3.9 %collective-permute-start.1 = (f32[40,64]{1,0:T(8,128)S(1)}, f32[40,64]{1,0:T(8,128)S(1)}, u32[]{:S(2)}, u32[]{:S(2)}) collective-permute-start(f32[40,64]{1,0:T(8,128)S(1)} %pad_maximum_fusion.1), channel_id=1, source_target_pairs={{0,6},{1,7},{2,0},{3,1},{4,2},{5,3},{6,4},{7,5},{8,14},{9,15},{10,... | collective-permute-start | bytes 30728 | tf_op jit(solution)/shard_map/ppermute | solution.py:51
  62.8 4.4 %collective-permute-start.2 = (f32[40,64]{1,0:T(8,128)S(1)}, f32[40,64]{1,0:T(8,128)S(1)}, u32[]{:S(2)}, u32[]{:S(2)}) collective-permute-start(f32[40,64]{1,0:T(8,128)S(1)} %pad_maximum_fusion.1), channel_id=1, source_target_pairs={{0,4},{1,5},{2,6},{3,7},{4,0},{5,1},{6,2},{7,3},{8,12},{9,13},{10,... | collective-permute-start | bytes 30728 | tf_op jit(solution)/shard_map/ppermute | solution.py:51
  67.2 4.7 %collective-permute-start.3 = (f32[40,64]{1,0:T(8,128)S(1)}, f32[40,64]{1,0:T(8,128)S(1)}, u32[]{:S(2)}, u32[]{:S(2)}) collective-permute-start(f32[40,64]{1,0:T(8,128)S(1)} %pad_maximum_fusion.1), channel_id=1, source_target_pairs={{0,2},{1,3},{2,4},{3,5},{4,6},{5,7},{6,0},{7,1},{8,10},{9,11},{10,... | collective-permute-start | bytes 30728 | tf_op jit(solution)/shard_map/ppermute | solution.py:51
  72.5 15.3 %collective-permute-start.23 = (bf16[2,4,352,128]{3,2,1,0:T(8,128)(2,1)S(1)}, bf16[2,4,352,128]{3,2,1,0:T(8,128)(2,1)S(1)}, u32[]{:S(2)}, u32[]{:S(2)}) collective-permute-start(bf16[2,4,352,128]{3,2,1,0:T(8,128)(2,1)S(1)} %get-tuple-element.34.refs_3_.refs_1_), channel_id=1, source_target_pairs={{0,6},{1,7},{2,0},{3,1},{4,2},{5,3},{6,4},{7,5},{8,14},{9,15},{10,... | collective-permute-start | bytes 2162696 | tf_op jit(solution)/shard_map/ppermute | solution.py:51
  74.0 34.3 %copy-start.13 = (bf16[128,2048]{1,0:T(8,128)(2,1)}, bf16[128,2048]{1,0:T(8,128)(2,1)S(1)}, u32[]{:S(2)}) copy-start(bf16[128,2048]{1,0:T(8,128)(2,1)S(1)} %collective-permute-done) | copy-start | bytes 1572868
  74.0 29.3 %collective-permute-start.22 = (bf16[2,4,352,128]{3,2,1,0:T(8,128)(2,1)S(1)}, bf16[2,4,352,128]{3,2,1,0:T(8,128)(2,1)}, u32[]{:S(2)}, u32[]{:S(2)}) collective-permute-start(bf16[2,4,352,128]{3,2,1,0:T(8,128)(2,1)S(1)} %shard_map.142.refs_2_.refs_0_), channel_id=1, source_target_pairs={{0,6},{1,7},{2,0},{3,1},{4,2},{5,3},{6,4},{7,5},{8,14},{9,15},{10,... | collective-permute-start | bytes 2162696 | tf_op jit(solution)/shard_map/ppermute | solution.py:51
  74.1 29.2 %collective-permute-start.27 = (bf16[2,4,352,128]{3,2,1,0:T(8,128)(2,1)S(1)}, bf16[2,4,352,128]{3,2,1,0:T(8,128)(2,1)S(1)}, u32[]{:S(2)}, u32[]{:S(2)}) collective-permute-start(bf16[2,4,352,128]{3,2,1,0:T(8,128)(2,1)S(1)} %shard_map.142.refs_2_.refs_0_), channel_id=1, source_target_pairs={{0,2},{1,3},{2,4},{3,5},{4,6},{5,7},{6,0},{7,1},{8,10},{9,11},{10,... | collective-permute-start | bytes 2162696 | tf_op jit(solution)/shard_map/ppermute | solution.py:51
  88.7 19.7 %collective-permute-start.26 = (bf16[2,4,352,128]{3,2,1,0:T(8,128)(2,1)S(1)}, bf16[2,4,352,128]{3,2,1,0:T(8,128)(2,1)S(1)}, u32[]{:S(2)}, u32[]{:S(2)}) collective-permute-start(bf16[2,4,352,128]{3,2,1,0:T(8,128)(2,1)S(1)} %collective-permute-done.25.refs_9_.refs_7_), channel_id=1, source_target_pairs={{0,2},{1,3},{2,4},{3,5},{4,6},{5,7},{6,0},{7,1},{8,10},{9,11},{10,... | collective-permute-start | bytes 2162696 | tf_op jit(solution)/shard_map/ppermute | solution.py:51
  103.3 24.7 %collective-permute-start.11 = (bf16[2,4,704,128]{3,2,1,0:T(8,128)(2,1)}, bf16[2,4,704,128]{3,2,1,0:T(8,128)(2,1)}, u32[]{:S(2)}, u32[]{:S(2)}) collective-permute-start(bf16[2,4,704,128]{3,2,1,0:T(8,128)(2,1)} %get-tuple-element.31.refs_1_), channel_id=1, source_target_pairs={{0,224},{1,25},{2,226},{3,27},{4,228},{5,29},{6,230},{7,31},{8,232... | collective-permute-start | bytes 4325384 | tf_op jit(solution)/shard_map/ppermute | solution.py:51
  104.2 24.0 %collective-permute-start.12 = (bf16[2,4,704,128]{3,2,1,0:T(8,128)(2,1)S(1)}, bf16[2,4,704,128]{3,2,1,0:T(8,128)(2,1)}, u32[]{:S(2)}, u32[]{:S(2)}) collective-permute-start(bf16[2,4,704,128]{3,2,1,0:T(8,128)(2,1)S(1)} %shard_map.138.refs_0_), channel_id=1, source_target_pairs={{0,32},{1,9},{2,34},{3,11},{4,36},{5,13},{6,38},{7,15},{8,40},{9,1... | collective-permute-start | bytes 4325384 | tf_op jit(solution)/shard_map/ppermute | solution.py:51
  105.7 33.5 %collective-permute-start.15 = (bf16[2,4,704,128]{3,2,1,0:T(8,128)(2,1)}, bf16[2,4,704,128]{3,2,1,0:T(8,128)(2,1)}, u32[]{:S(2)}, u32[]{:S(2)}) collective-permute-start(bf16[2,4,704,128]{3,2,1,0:T(8,128)(2,1)} %collective-permute-done.13.refs_5_), channel_id=1, source_target_pairs={{0,32},{1,9},{2,34},{3,11},{4,36},{5,13},{6,38},{7,15},{8,40},{9,1... | collective-permute-start | bytes 4325384 | tf_op jit(solution)/shard_map/ppermute | solution.py:51
  105.7 34.0 %collective-permute-start.14 = (bf16[2,4,704,128]{3,2,1,0:T(8,128)(2,1)}, bf16[2,4,704,128]{3,2,1,0:T(8,128)(2,1)}, u32[]{:S(2)}, u32[]{:S(2)}) collective-permute-start(bf16[2,4,704,128]{3,2,1,0:T(8,128)(2,1)} %collective-permute-done.10.refs_2_), channel_id=1, source_target_pairs={{0,224},{1,25},{2,226},{3,27},{4,228},{5,29},{6,230},{7,31},{8,232... | collective-permute-start | bytes 4325384 | tf_op jit(solution)/shard_map/ppermute | solution.py:51
  109.2 13.6 %collective-permute-start.24 = (bf16[2,4,352,128]{3,2,1,0:T(8,128)(2,1)}, bf16[2,4,352,128]{3,2,1,0:T(8,128)(2,1)}, u32[]{:S(2)}, u32[]{:S(2)}) collective-permute-start(bf16[2,4,352,128]{3,2,1,0:T(8,128)(2,1)} %collective-permute-done.22.refs_4_.refs_2_), channel_id=1, source_target_pairs={{0,6},{1,7},{2,0},{3,1},{4,2},{5,3},{6,4},{7,5},{8,14},{9,15},{10,... | collective-permute-start | bytes 2162696 | tf_op jit(solution)/shard_map/ppermute | solution.py:51
  111.6 16.5 %copy-start.9 = (bf16[4,4,352,128]{3,2,1,0:T(8,128)(2,1)S(1)}, bf16[4,4,352,128]{3,2,1,0:T(8,128)(2,1)}, u32[]{:S(2)}) copy-start(bf16[4,4,352,128]{3,2,1,0:T(8,128)(2,1)} %copy-done.8) | copy-start | bytes 4325380
  122.9 32.1 %collective-permute-start.32 = (bf16[4,4,160,128]{3,2,1,0:T(8,128)(2,1)S(1)}, bf16[4,4,160,128]{3,2,1,0:T(8,128)(2,1)S(1)}, u32[]{:S(2)}, u32[]{:S(2)}) collective-permute-start(bf16[4,4,160,128]{3,2,1,0:T(8,128)(2,1)S(1)} %get-tuple-element.39.refs_4_.refs_0_), channel_id=1, source_target_pairs={{0,6},{1,7},{2,0},{3,1},{4,2},{5,3},{6,4},{7,5},{8,14},{9,15},{10,... | collective-permute-start | bytes 1966088 | tf_op jit(solution)/shard_map/ppermute | solution.py:51
  128.1 34.6 %collective-permute-start.33 = (bf16[4,4,160,128]{3,2,1,0:T(8,128)(2,1)S(1)}, bf16[4,4,160,128]{3,2,1,0:T(8,128)(2,1)S(1)}, u32[]{:S(2)}, u32[]{:S(2)}) collective-permute-start(bf16[4,4,160,128]{3,2,1,0:T(8,128)(2,1)S(1)} %get-tuple-element.39.refs_4_.refs_0_), channel_id=1, source_target_pairs={{0,4},{1,5},{2,6},{3,7},{4,0},{5,1},{6,2},{7,3},{8,12},{9,13},{10,... | collective-permute-start | bytes 1966088 | tf_op jit(solution)/shard_map/ppermute | solution.py:51
  128.2 19.3 %copy-start.1 = (bf16[2,4,352,128]{3,2,1,0:T(8,128)(2,1)S(1)}, bf16[2,4,352,128]{3,2,1,0:T(8,128)(2,1)}, u32[]{:S(2)}) copy-start(bf16[2,4,352,128]{3,2,1,0:T(8,128)(2,1)} %copy-done) | copy-start | bytes 2162692
  128.2 19.3 %copy-start.3 = (bf16[2,4,352,128]{3,2,1,0:T(8,128)(2,1)S(1)}, bf16[2,4,352,128]{3,2,1,0:T(8,128)(2,1)}, u32[]{:S(2)}) copy-start(bf16[2,4,352,128]{3,2,1,0:T(8,128)(2,1)} %copy-done.2) | copy-start | bytes 2162692
  128.2 19.3 %copy-start.5 = (bf16[2,4,352,128]{3,2,1,0:T(8,128)(2,1)S(1)}, bf16[2,4,352,128]{3,2,1,0:T(8,128)(2,1)}, u32[]{:S(2)}) copy-start(bf16[2,4,352,128]{3,2,1,0:T(8,128)(2,1)} %copy-done.4) | copy-start | bytes 2162692
  128.2 19.3 %copy-start.7 = (bf16[2,4,352,128]{3,2,1,0:T(8,128)(2,1)S(1)}, bf16[2,4,352,128]{3,2,1,0:T(8,128)(2,1)}, u32[]{:S(2)}) copy-start(bf16[2,4,352,128]{3,2,1,0:T(8,128)(2,1)} %copy-done.6) | copy-start | bytes 2162692
  128.2 51.9 %collective-permute-start.29 = (bf16[4,4,352,128]{3,2,1,0:T(8,128)(2,1)S(1)}, bf16[4,4,352,128]{3,2,1,0:T(8,128)(2,1)S(1)}, u32[]{:S(2)}, u32[]{:S(2)}) collective-permute-start(bf16[4,4,352,128]{3,2,1,0:T(8,128)(2,1)S(1)} %copy-done.9), channel_id=1, source_target_pairs={{0,224},{1,25},{2,226},{3,27},{4,228},{5,29},{6,230},{7,31},{8,232... | collective-permute-start | bytes 4325384 | tf_op jit(solution)/shard_map/ppermute | solution.py:51
  139.1 41.0 %collective-permute-start.30 = (bf16[4,4,352,128]{3,2,1,0:T(8,128)(2,1)S(1)}, bf16[4,4,352,128]{3,2,1,0:T(8,128)(2,1)S(1)}, u32[]{:S(2)}, u32[]{:S(2)}) collective-permute-start(bf16[4,4,352,128]{3,2,1,0:T(8,128)(2,1)S(1)} %copy-done.9), channel_id=1, source_target_pairs={{0,192},{1,17},{2,194},{3,19},{4,196},{5,21},{6,198},{7,23},{8,200... | collective-permute-start | bytes 4325384 | tf_op jit(solution)/shard_map/ppermute | solution.py:51
  139.7 40.4 %collective-permute-start.31 = (bf16[4,4,352,128]{3,2,1,0:T(8,128)(2,1)S(1)}, bf16[4,4,352,128]{3,2,1,0:T(8,128)(2,1)S(1)}, u32[]{:S(2)}, u32[]{:S(2)}) collective-permute-start(bf16[4,4,352,128]{3,2,1,0:T(8,128)(2,1)S(1)} %copy-done.9), channel_id=1, source_target_pairs={{0,32},{1,9},{2,34},{3,11},{4,36},{5,13},{6,38},{7,15},{8,40},{9,1... | collective-permute-start | bytes 4325384 | tf_op jit(solution)/shard_map/ppermute | solution.py:51
  147.5 15.7 %copy-start.18 = (f32[3,2048]{1,0:T(4,128)S(1)}, f32[3,2048]{1,0:T(4,128)}, u32[]{:S(2)}) copy-start(f32[3,2048]{1,0:T(4,128)} %param.27) | copy-start | bytes 73732
  147.5 32.6 %copy-start.10 = (bf16[2048,32]{0,1:T(8,128)(2,1)S(1)}, bf16[2048,32]{0,1:T(8,128)(2,1)}, u32[]{:S(2)}) copy-start(bf16[2048,32]{0,1:T(8,128)(2,1)} %param.22) | copy-start | bytes 393220
  155.0 25.1 %collective-permute-start.28 = (bf16[256,2048]{1,0:T(8,128)(2,1)S(1)}, bf16[256,2048]{1,0:T(8,128)(2,1)S(1)}, u32[]{:S(2)}, u32[]{:S(2)}) collective-permute-start(bf16[256,2048]{1,0:T(8,128)(2,1)S(1)} %get-tuple-element.35.mine_ref), channel_id=1, source_target_pairs={{0,1},{1,0},{2,3},{3,2},{4,5},{5,4},{6,7},{7,6},{8,9},{9,8},{10,11... | collective-permute-start | bytes 3145736 | tf_op jit(solution)/shard_map/ppermute | solution.py:430
  162.7 17.4 %collective-permute-start.34 = (bf16[4,4,160,128]{3,2,1,0:T(8,128)(2,1)S(1)}, bf16[4,4,160,128]{3,2,1,0:T(8,128)(2,1)S(1)}, u32[]{:S(2)}, u32[]{:S(2)}) collective-permute-start(bf16[4,4,160,128]{3,2,1,0:T(8,128)(2,1)S(1)} %get-tuple-element.39.refs_4_.refs_0_), channel_id=1, source_target_pairs={{0,2},{1,3},{2,4},{3,5},{4,6},{5,7},{6,0},{7,1},{8,10},{9,11},{10,... | collective-permute-start | bytes 1966088 | tf_op jit(solution)/shard_map/ppermute | solution.py:51
  187.8 13.4 %collective-permute-start.35 = (f32[136,256]{1,0:T(8,128)S(1)}, f32[136,256]{1,0:T(8,128)S(1)}, u32[]{:S(2)}, u32[]{:S(2)}) collective-permute-start(f32[136,256]{1,0:T(8,128)S(1)} %get-tuple-element.47), channel_id=1, source_target_pairs={{0,2},{2,4},{4,6},{1,3},{3,5},{5,7},{8,10},{10,12},{12,14},{9,11},... | collective-permute-start | bytes 417800 | tf_op jit(solution)/shard_map/ppermute | solution.py:505
  189.1 12.1 %collective-permute-start.36 = (f32[136,256]{1,0:T(8,128)S(1)}, f32[136,256]{1,0:T(8,128)S(1)}, u32[]{:S(2)}, u32[]{:S(2)}) collective-permute-start(f32[136,256]{1,0:T(8,128)S(1)} %get-tuple-element.47), channel_id=1, source_target_pairs={{0,4},{2,6},{1,5},{3,7},{8,12},{10,14},{9,13},{11,15},{16,20},{18,... | collective-permute-start | bytes 417800 | tf_op jit(solution)/shard_map/ppermute | solution.py:505
  194.3 6.9 %collective-permute-start.37 = (f32[136,256]{1,0:T(8,128)S(1)}, f32[136,256]{1,0:T(8,128)S(1)}, u32[]{:S(2)}, u32[]{:S(2)}) collective-permute-start(f32[136,256]{1,0:T(8,128)S(1)} %get-tuple-element.47), channel_id=1, source_target_pairs={{0,6},{1,7},{8,14},{9,15},{16,22},{17,23},{24,30},{25,31},{32,38},... | collective-permute-start | bytes 417800 | tf_op jit(solution)/shard_map/ppermute | solution.py:505
  203.9 3.9 %collective-permute-start.38 = (bf16[256,2048]{1,0:T(8,128)(2,1)S(1)}, bf16[256,2048]{1,0:T(8,128)(2,1)S(1)}, u32[]{:S(2)}, u32[]{:S(2)}) collective-permute-start(bf16[256,2048]{1,0:T(8,128)(2,1)S(1)} %shard_map.147.mine_ref), channel_id=1, source_target_pairs={{0,1},{1,0},{2,3},{3,2},{4,5},{5,4},{6,7},{7,6},{8,9},{9,8},{10,11... | collective-permute-start | bytes 3145736 | tf_op jit(solution)/shard_map/ppermute | solution.py:430
  218.0 2.0 collective-permute-start.39
  (13 other events, 46.7 us)
